TPU v7x, 512 devices: a whole 4x4x16 slice. The times are simulated.
512 devices in a mesh: kv: 16 (over y, x), tp: 32 (over z, core).
Axes of the slice: x: 4, y: 4, z: 16, core: 2. Of those that a mesh axis runs over, the one named last changes fastest.
Arguments:
- hidden_in: bfloat16 [64, 4096], P('kv', 'tp'), may hold values from -12 to 12
- mixer_gain: float32 [4096], P('tp'), may hold values from 0.1 to 1.9
- query_weight: bfloat16 [4096, 4096], P('tp', 'kv'), may hold values from -0.09375 to 0.09375
- key_weight: bfloat16 [4096, 4096], P('tp', 'kv'), may hold values from -0.09375 to 0.09375
- value_weight: bfloat16 [4096, 8192], P('tp', 'kv'), may hold values from -0.09375 to 0.09375
- gate_weight: bfloat16 [4096, 8192], P('tp', 'kv'), may hold values from -0.09375 to 0.09375
- decay_rate: float32 [16], P('kv'), may hold values from 0.0005 to 0.15
- prior_state: float32 [64, 16, 256, 512], P('tp', 'kv'), may hold values from -2.5 to 2.5
- key_block: bfloat16 [64, 16, 128, 256], P('tp', 'kv'), may hold values from -1 to 1
- value_block: bfloat16 [64, 16, 128, 512], P('tp', 'kv'), may hold values from -6 to 6
- lengths: int32 [64], P('tp'), may hold values from 1 to 16384, 262144 in all
- group_gain: float32 [8192], P('kv'), may hold values from 0.1 to 1.9
- output_weight: bfloat16 [8192, 4096], P('kv', 'tp'), may hold values from -0.0625 to 0.0625
- channel_gain: float32 [4096], P('tp'), may hold values from 0.1 to 1.9
- hidden_gate: bfloat16 [4096, 11264], P('tp', 'kv'), may hold values from -0.09375 to 0.09375
- hidden_up: bfloat16 [4096, 11264], P('tp', 'kv'), may hold values from -0.09375 to 0.09375
- hidden_down: bfloat16 [11264, 4096], P('kv', 'tp'), may hold values from -0.0546875 to 0.0546875
Outputs:
- layer_out: bfloat16 [64, 4096], P('kv', 'tp')
Inputs may be any that keep to these rules, and one draw needn't show every extreme that they name: Sequence s has lengths[s] earlier positions; slots 0 to (lengths[s] mod 128) - 1 of key_block and value_block hold the turned, scaled keys and the values of its positions from 128 * floor(lengths[s] / 128) on, prior_state holds the state of the positions before them, and the other slots take no part.
All inputs are finite; a program needn't handle non-finite values. No bound on the sum of `lengths` on one device may be relied on, other than what follows from the above.
Results may differ from a plain program's by a relative error of at most 0.029.
Values may be sent and summed in bfloat16 or wider, within the bound.
A program may use at most 64 MiB of HBM per device.

v0:
```python
import jax
import jax.numpy as jnp
from jax import lax
from jax.sharding import PartitionSpec as P

D = 4096


epsilon = 1e-06


def from_everyone(value, axis):
    copies = jnp.broadcast_to(value, (lax.axis_size(axis), *value.shape))
    return lax.all_to_all(copies, axis, split_axis=0, concat_axis=0, tiled=True)


def over_copies(value, axis):
    return from_everyone(value, axis).sum(axis=0)


def in_order(parts, dim):
    shape = list(parts.shape[1:])
    shape[dim] *= parts.shape[0]
    return jnp.moveaxis(parts, 0, dim).reshape(shape)


def gathered_copies(value, axis, dim):
    parts = from_everyone(value, axis)
    return in_order(parts, dim)


def split_up(value, dim, count):
    shape = value.shape
    parts = value.reshape(*shape[:dim], count, shape[dim] // count, *shape[dim + 1 :])
    return jnp.moveaxis(parts, dim, 0)


def summed_on_arrival(value, axis, dim):
    count = lax.axis_size(axis)
    parts = lax.all_to_all(split_up(value, dim, count), axis, 0, 0, tiled=True)
    return jnp.sum(parts.astype(jnp.float32), axis=0)


def as_sent(value):
    return jax.tree.map(lambda a: a.astype(jnp.bfloat16) if a.dtype == jnp.float32 else a, value)


def side_by_side(arrays, axis, dim, along):
    ends, at = ([], 0)
    for a in arrays[:-1]:
        at += a.shape[along]
        ends.append(at)
    both = jnp.concatenate(arrays, axis=along)
    return tuple(jnp.split(summed_on_arrival(both, axis, dim), ends, axis=along))


def rotate(vectors, position):
    half_dim = vectors.shape[-1] // 2
    inverse = 10000.0 ** (-jnp.arange(half_dim, dtype=jnp.float32) / half_dim)
    angles = position.astype(jnp.float32)[:, None, None] * inverse
    cosine_part = jnp.cos(angles)
    sine_part = jnp.sin(angles)
    front_half = vectors[..., :half_dim]
    back_half = vectors[..., half_dim:]
    return jnp.concatenate(
        [
            front_half * cosine_part - back_half * sine_part,
            front_half * sine_part + back_half * cosine_part,
        ],
        axis=-1,
    )


def retain(
    queries,
    keys_new,
    values_new,
    gates,
    decay_rate,
    prior_state,
    key_block,
    value_block,
    lengths,
    group_gain,
):
    batch_rows = queries.shape[0]
    heads_here = decay_rate.shape[0]
    key_width = prior_state.shape[2]
    value_width = prior_state.shape[3]
    block_len = key_block.shape[2]
    rotated = rotate(
        queries.astype(jnp.float32).reshape(batch_rows, heads_here, key_width), lengths
    ).astype(jnp.bfloat16)
    fresh_keys = rotate(
        keys_new.astype(jnp.float32).reshape(batch_rows, heads_here, key_width), lengths
    ) * key_width ** (-0.5)
    fresh_values = values_new.astype(jnp.float32).reshape(batch_rows, heads_here, value_width)
    filled = lengths % block_len
    slots = jnp.arange(block_len, dtype=jnp.int32)
    distance = (filled[:, None] - slots[None, :]).astype(jnp.float32)
    live_slots = (slots[None, :] < filled[:, None])[:, None, :]
    weighting = jnp.where(
        live_slots, jnp.exp(-decay_rate[None, :, None] * distance[:, None, :]), jnp.float32(0.0)
    )
    scores = jnp.einsum("shk,shjk->shj", rotated, key_block, preferred_element_type=jnp.float32)
    block_weights = (scores * weighting).astype(jnp.bfloat16)
    block_term = jnp.einsum(
        "shj,shjv->shv", block_weights, value_block, preferred_element_type=jnp.float32
    )
    rotated_wide = rotated.astype(jnp.float32)
    own_term = jnp.sum(rotated_wide * fresh_keys, axis=-1, keepdims=True) * fresh_values
    carried = jnp.exp(-decay_rate[None, :, None] * (filled[:, None, None] + 1).astype(jnp.float32))
    state_term = carried * jnp.einsum(
        "shk,shkv->shv", rotated_wide, prior_state, precision=lax.Precision.HIGHEST
    )
    retained = own_term + block_term + state_term
    centre = jnp.mean(retained, axis=-1, keepdims=True)
    spread = jnp.mean(jnp.square(retained - centre), axis=-1, keepdims=True)
    normed = (retained - centre) * lax.rsqrt(spread + epsilon)
    gated = (
        jax.nn.silu(gates.astype(jnp.float32)).reshape(batch_rows, heads_here, value_width)
        * normed
        * group_gain.reshape(heads_here, value_width)
    )
    return gated.astype(jnp.bfloat16).reshape(batch_rows, heads_here * value_width)


def local(
    hidden_in,
    mixer_gain,
    query_weight,
    key_weight,
    value_weight,
    gate_weight,
    decay_rate,
    prior_state,
    key_block,
    value_block,
    lengths,
    group_gain,
    output_weight,
    channel_gain,
    hidden_gate,
    hidden_up,
    hidden_down,
):
    local_seqs = lengths.shape[0]
    first_row = lax.axis_index("tp") * local_seqs
    stream = hidden_in.astype(jnp.float32)
    scaled_in = (stream * mixer_gain).astype(jnp.bfloat16)
    own_squares = jnp.sum(stream * stream, axis=1)
    own_squares = over_copies(own_squares, "tp")
    all_rows, all_squares = (
        gathered_copies(scaled_in, "kv", 0),
        gathered_copies(own_squares.astype(jnp.bfloat16), "kv", 0).astype(own_squares.dtype),
    )
    weights_in = (query_weight, key_weight, value_weight, gate_weight)
    terms = tuple(
        (jnp.dot(all_rows, matrix, preferred_element_type=jnp.float32) for matrix in weights_in)
    )
    summed = jax.tree.map(lambda part: summed_on_arrival(part, "tp", 0), as_sent(terms))
    row_squares = lax.dynamic_slice_in_dim(all_squares, first_row, local_seqs, 0)
    first_scale = lax.rsqrt(row_squares / D + epsilon)[:, None]
    queries = (first_scale * summed[0]).astype(jnp.bfloat16)
    keys_new = (first_scale * summed[1]).astype(jnp.bfloat16)
    values_new = (first_scale * summed[2]).astype(jnp.bfloat16)
    gates = (first_scale * summed[3]).astype(jnp.bfloat16)
    mixed = retain(
        queries,
        keys_new,
        values_new,
        gates,
        decay_rate,
        prior_state,
        key_block,
        value_block,
        lengths,
        group_gain,
    )
    head_terms = jnp.dot(
        gathered_copies(mixed, "tp", 0), output_weight, preferred_element_type=jnp.float32
    )
    mixer_out = summed_on_arrival(head_terms.astype(jnp.bfloat16), "kv", 0)
    middle = stream + mixer_out
    scaled_mid = (middle * channel_gain).astype(jnp.bfloat16)
    middle_squares = jnp.sum(middle * middle, axis=1)
    middle_squares = over_copies(middle_squares, "tp")
    middle_rows, middle_all = (
        gathered_copies(scaled_mid, "kv", 0),
        gathered_copies(middle_squares.astype(jnp.bfloat16), "kv", 0).astype(middle_squares.dtype),
    )
    channel_terms = (
        jnp.dot(middle_rows, hidden_gate, preferred_element_type=jnp.float32),
        jnp.dot(middle_rows, hidden_up, preferred_element_type=jnp.float32),
    )
    channel_summed = side_by_side(
        (channel_terms[0].astype(jnp.bfloat16), channel_terms[1].astype(jnp.bfloat16)), "tp", 0, 1
    )
    middle_row_squares = lax.dynamic_slice_in_dim(middle_all, first_row, local_seqs, 0)
    second_scale = lax.rsqrt(middle_row_squares / D + epsilon)[:, None]
    gate_part = second_scale * channel_summed[0]
    up_part = second_scale * channel_summed[1]
    activated = (jax.nn.silu(gate_part) * up_part).astype(jnp.bfloat16)
    unit_terms = jnp.dot(
        gathered_copies(activated, "tp", 0), hidden_down, preferred_element_type=jnp.float32
    )
    channel_out = summed_on_arrival(unit_terms.astype(jnp.bfloat16), "kv", 0)
    return (middle + channel_out).astype(jnp.bfloat16)


def solution(mesh):
    in_specs = (
        P("kv", "tp"),
        P("tp"),
        P("tp", "kv"),
        P("tp", "kv"),
        P("tp", "kv"),
        P("tp", "kv"),
        P("kv"),
        P("tp", "kv", None, None),
        P("tp", "kv", None, None),
        P("tp", "kv", None, None),
        P("tp"),
        P("kv"),
        P("kv", "tp"),
        P("tp"),
        P("tp", "kv"),
        P("tp", "kv"),
        P("kv", "tp"),
    )
    out_specs = P("kv", "tp")
    return jax.shard_map(local, mesh=mesh, in_specs=in_specs, out_specs=out_specs, check_vma=False)
```

profile of v0, /device:TPU:1, one launch (start us, length us, event | category | flops | bytes accessed | tf_op | source)
XLA Modules:
  0.0 247.6 jit_solution(4408424907867211999)
XLA Ops:
  0.0 0.9 fusion.12
  0.9 0.6 broadcast_in_dim.20
  1.5 16.7 %all-to-all-start = ((f32[32,1,4]{2,1,0:T(1,128)}), f32[32,1,4]{2,1,0:T(1,128)S(1)}, u32[]{:S(2)}, u32[]{:S(2)}) async-start(f32[32,1,4]{2,1,0:T(1,128)} %broadcast_in_dim.20), calls=%async_computation | async-start | bytes 32768 | tf_op jit(solution)/shard_map/all_to_all | solution.py:14
  18.9 0.6 copy-done.14
  19.6 10.4 %all-to-all-done = f32[32,1,4]{2,1,0:T(1,128)S(1)} async-done(((f32[32,1,4]{2,1,0:T(1,128)}), f32[32,1,4]{2,1,0:T(1,128)S(1)}, u32[]{:S(2)}, u32[]{:S(2)}) %all-to-all-start) | async-done | bytes 544 | tf_op jit(solution)/shard_map/all_to_all | solution.py:14
  30.1 0.6 broadcast_in_dim.21
  30.7 6.8 %all-to-all-start.1 = ((bf16[16,1,4]{2,1,0:T(2,128)(2,1)}), bf16[16,1,4]{2,1,0:T(2,128)(2,1)S(1)}, u32[]{:S(2)}, u32[]{:S(2)}) async-start(bf16[16,1,4]{2,1,0:T(2,128)(2,1)} %broadcast_in_dim.21), calls=%async_computation.1 | async-start | bytes 16384 | tf_op jit(solution)/shard_map/all_to_all | solution.py:14
  37.4 6.4 %all-to-all-done.1 = bf16[16,1,4]{2,1,0:T(2,128)(2,1)S(1)} async-done(((bf16[16,1,4]{2,1,0:T(2,128)(2,1)}), bf16[16,1,4]{2,1,0:T(2,128)(2,1)S(1)}, u32[]{:S(2)}, u32[]{:S(2)}) %all-to-all-start.1) | async-done | bytes 160 | tf_op jit(solution)/shard_map/all_to_all | solution.py:14
  43.9 0.6 broadcast_in_dim.22
  44.5 3.5 %all-to-all-start.2 = ((bf16[16,4,128]{2,1,0:T(4,128)(2,1)}), bf16[16,4,128]{2,1,0:T(4,128)(2,1)S(1)}, u32[]{:S(2)}, u32[]{:S(2)}) async-start(bf16[16,4,128]{2,1,0:T(4,128)(2,1)} %broadcast_in_dim.22), calls=%async_computation.2 | async-start | bytes 32768 | tf_op jit(solution)/shard_map/all_to_all | solution.py:14
  48.2 6.2 %all-to-all-done.2 = bf16[16,4,128]{2,1,0:T(4,128)(2,1)S(1)} async-done(((bf16[16,4,128]{2,1,0:T(4,128)(2,1)}), bf16[16,4,128]{2,1,0:T(4,128)(2,1)S(1)}, u32[]{:S(2)}, u32[]{:S(2)}) %all-to-all-start.2) | async-done | bytes 16416 | tf_op jit(solution)/shard_map/all_to_all | solution.py:14
  54.5 0.6 reshape.373
  55.1 7.0 %all-to-all-start.5 = ((bf16[32,2,256]{2,1,0:T(2,128)(2,1)}), bf16[32,2,256]{2,1,0:T(2,128)(2,1)S(1)}, u32[]{:S(2)}, u32[]{:S(2)}) async-start(bf16[32,2,256]{2,1,0:T(2,128)(2,1)} %reshape.373), calls=%async_computation.5 | async-start | bytes 65536 | tf_op jit(solution)/shard_map/all_to_all | solution.py:40
  62.2 0.6 reshape.372
  63.0 11.3 %all-to-all-done.5 = bf16[32,2,256]{2,1,0:T(2,128)(2,1)S(1)} async-done(((bf16[32,2,256]{2,1,0:T(2,128)(2,1)}), bf16[32,2,256]{2,1,0:T(2,128)(2,1)S(1)}, u32[]{:S(2)}, u32[]{:S(2)}) %all-to-all-start.5) | async-done | bytes 32800 | tf_op jit(solution)/shard_map/all_to_all | solution.py:40
  74.4 4.5 %all-to-all-start.4 = ((bf16[32,2,256]{2,1,0:T(2,128)(2,1)}), bf16[32,2,256]{2,1,0:T(2,128)(2,1)S(1)}, u32[]{:S(2)}, u32[]{:S(2)}) async-start(bf16[32,2,256]{2,1,0:T(2,128)(2,1)} %reshape.372), calls=%async_computation.4 | async-start | bytes 65536 | tf_op jit(solution)/shard_map/all_to_all | solution.py:40
  79.1 0.7 reshape.374
  79.7 0.6 reshape.371
  80.4 10.7 %all-to-all-done.4 = bf16[32,2,256]{2,1,0:T(2,128)(2,1)S(1)} async-done(((bf16[32,2,256]{2,1,0:T(2,128)(2,1)}), bf16[32,2,256]{2,1,0:T(2,128)(2,1)S(1)}, u32[]{:S(2)}, u32[]{:S(2)}) %all-to-all-start.4) | async-done | bytes 32800 | tf_op jit(solution)/shard_map/all_to_all | solution.py:40
  91.1 4.5 %all-to-all-start.6 = ((bf16[32,2,512]{2,1,0:T(2,128)(2,1)}), bf16[32,2,512]{2,1,0:T(2,128)(2,1)S(1)}, u32[]{:S(2)}, u32[]{:S(2)}) async-start(bf16[32,2,512]{2,1,0:T(2,128)(2,1)} %reshape.374), calls=%async_computation.6 | async-start | bytes 131072 | tf_op jit(solution)/shard_map/all_to_all | solution.py:40
  96.2 0.2 fusion.2
  96.5 0.4 fusion
  96.9 11.8 %all-to-all-done.6 = bf16[32,2,512]{2,1,0:T(2,128)(2,1)S(1)} async-done(((bf16[32,2,512]{2,1,0:T(2,128)(2,1)}), bf16[32,2,512]{2,1,0:T(2,128)(2,1)S(1)}, u32[]{:S(2)}, u32[]{:S(2)}) %all-to-all-start.6) | async-done | bytes 65568 | tf_op jit(solution)/shard_map/all_to_all | solution.py:40
  108.7 5.1 %all-to-all-start.3 = ((bf16[32,2,512]{2,1,0:T(2,128)(2,1)}), bf16[32,2,512]{2,1,0:T(2,128)(2,1)S(1)}, u32[]{:S(2)}, u32[]{:S(2)}) async-start(bf16[32,2,512]{2,1,0:T(2,128)(2,1)} %reshape.371), calls=%async_computation.3 | async-start | bytes 131072 | tf_op jit(solution)/shard_map/all_to_all | solution.py:40
  113.9 0.2 fusion.41
  114.1 0.2 multiply_reduce_fusion
  114.3 12.5 %all-to-all-done.3 = bf16[32,2,512]{2,1,0:T(2,128)(2,1)S(1)} async-done(((bf16[32,2,512]{2,1,0:T(2,128)(2,1)}), bf16[32,2,512]{2,1,0:T(2,128)(2,1)S(1)}, u32[]{:S(2)}, u32[]{:S(2)}) %all-to-all-start.3) | async-done | bytes 65568 | tf_op jit(solution)/shard_map/all_to_all | solution.py:40
  127.1 17.4 %all_to_all.79 = bf16[32,2,512]{2,1,0:T(2,128)(2,1)S(1)} all-to-all(bf16[32,2,512]{2,1,0:T(2,128)(2,1)S(1)} %broadcast_in_dim.24), channel_id=1, replica_groups=mesh['kv'=16,'tp'=32] {'tp'}, dimensions={0} | all-to-all | bytes 131072 | tf_op jit(solution)/shard_map/all_to_all | solution.py:14
  144.6 0.2 convolution_convert_fusion.7
  144.7 9.2 %all_to_all.80 = bf16[16,4,128]{2,1,0:T(4,128)(2,1)S(1)} all-to-all(bf16[16,4,128]{2,1,0:T(4,128)(2,1)S(1)} %bitcast.67), channel_id=1, replica_groups=mesh['kv'=16,'tp'=32] {'kv'}, dimensions={0} | all-to-all | bytes 32768 | tf_op jit(solution)/shard_map/all_to_all | solution.py:40
  154.0 0.6 copy-done.11
  154.8 17.6 %all_to_all.81 = f32[32,1,4]{2,1,0:T(1,128)S(1)} all-to-all(f32[32,1,4]{2,1,0:T(1,128)S(1)} %broadcast_in_dim.25), channel_id=1, replica_groups=mesh['kv'=16,'tp'=32] {'tp'}, dimensions={0} | all-to-all | bytes 1024 | tf_op jit(solution)/shard_map/all_to_all | solution.py:14
  172.4 0.6 broadcast_in_dim.27
  173.0 3.6 %all-to-all-start.11 = ((bf16[16,4,128]{2,1,0:T(4,128)(2,1)}), bf16[16,4,128]{2,1,0:T(4,128)(2,1)S(1)}, u32[]{:S(2)}, u32[]{:S(2)}) async-start(bf16[16,4,128]{2,1,0:T(4,128)(2,1)} %broadcast_in_dim.27), calls=%async_computation.11 | async-start | bytes 32768 | tf_op jit(solution)/shard_map/all_to_all | solution.py:14
  176.7 6.3 %all-to-all-done.11 = bf16[16,4,128]{2,1,0:T(4,128)(2,1)S(1)} async-done(((bf16[16,4,128]{2,1,0:T(4,128)(2,1)}), bf16[16,4,128]{2,1,0:T(4,128)(2,1)S(1)}, u32[]{:S(2)}, u32[]{:S(2)}) %all-to-all-start.11) | async-done | bytes 16416 | tf_op jit(solution)/shard_map/all_to_all | solution.py:14
  183.0 0.6 broadcast_in_dim.26
  183.6 3.4 %all-to-all-start.10 = ((bf16[16,1,4]{2,1,0:T(2,128)(2,1)}), bf16[16,1,4]{2,1,0:T(2,128)(2,1)S(1)}, u32[]{:S(2)}, u32[]{:S(2)}) async-start(bf16[16,1,4]{2,1,0:T(2,128)(2,1)} %broadcast_in_dim.26), calls=%async_computation.10 | async-start | bytes 16384 | tf_op jit(solution)/shard_map/all_to_all | solution.py:14
  187.0 0.2 convolution_convert_fusion
  187.3 0.2 convolution_convert_fusion.1
  187.6 0.7 reshape.381
  188.3 5.0 %all-to-all-done.10 = bf16[16,1,4]{2,1,0:T(2,128)(2,1)S(1)} async-done(((bf16[16,1,4]{2,1,0:T(2,128)(2,1)}), bf16[16,1,4]{2,1,0:T(2,128)(2,1)S(1)}, u32[]{:S(2)}, u32[]{:S(2)}) %all-to-all-start.10) | async-done | bytes 160 | tf_op jit(solution)/shard_map/all_to_all | solution.py:14
  193.3 6.8 %all-to-all-start.12 = ((bf16[32,2,1408]{2,1,0:T(2,128)(2,1)}), bf16[32,2,1408]{2,1,0:T(2,128)(2,1)S(1)}, u32[]{:S(2)}, u32[]{:S(2)}) async-start(bf16[32,2,1408]{2,1,0:T(2,128)(2,1)} %reshape.381), calls=%async_computation.12 | async-start | bytes 360448 | tf_op jit(solution)/shard_map/all_to_all | solution.py:40
  200.3 17.8 %all-to-all-done.12 = bf16[32,2,1408]{2,1,0:T(2,128)(2,1)S(1)} async-done(((bf16[32,2,1408]{2,1,0:T(2,128)(2,1)}), bf16[32,2,1408]{2,1,0:T(2,128)(2,1)S(1)}, u32[]{:S(2)}, u32[]{:S(2)}) %all-to-all-start.12) | async-done | bytes 180256 | tf_op jit(solution)/shard_map/all_to_all | solution.py:40
  218.1 0.2 convert_reduce_fusion
  218.4 19.1 %all_to_all.82 = bf16[32,2,704]{2,1,0:T(2,128)(2,1)S(1)} all-to-all(bf16[32,2,704]{2,1,0:T(2,128)(2,1)S(1)} %broadcast_in_dim.28), channel_id=1, replica_groups=mesh['kv'=16,'tp'=32] {'tp'}, dimensions={0} | all-to-all | bytes 180224 | tf_op jit(solution)/shard_map/all_to_all | solution.py:14
  237.6 0.2 convolution_convert_fusion.6
  237.8 9.2 %all_to_all.83 = bf16[16,4,128]{2,1,0:T(4,128)(2,1)S(1)} all-to-all(bf16[16,4,128]{2,1,0:T(4,128)(2,1)S(1)} %bitcast.66), channel_id=1, replica_groups=mesh['kv'=16,'tp'=32] {'kv'}, dimensions={0} | all-to-all | bytes 32768 | tf_op jit(solution)/shard_map/all_to_all | solution.py:40
  247.0 0.6 add_convert_fusion
  (66 shorter events, 2.5 us)
Async XLA Ops:
  0.0 96.4 %copy-start = (f32[2,1,256,512]{3,2,1,0:T(8,128)S(1)}, f32[2,1,256,512]{3,2,1,0:T(8,128)}, u32[]{:S(2)}) copy-start(f32[2,1,256,512]{3,2,1,0:T(8,128)} %param.24) | copy-start | bytes 3145732
  1.5 28.5 %all-to-all-start = ((f32[32,1,4]{2,1,0:T(1,128)}), f32[32,1,4]{2,1,0:T(1,128)S(1)}, u32[]{:S(2)}, u32[]{:S(2)}) async-start(f32[32,1,4]{2,1,0:T(1,128)} %broadcast_in_dim.20), calls=%async_computation | async-start | bytes 32768 | tf_op jit(solution)/shard_map/all_to_all | solution.py:14
  18.9 0.7 copy-start.14
  19.6 34.7 %copy-start.9 = (bf16[128,256]{1,0:T(8,128)(2,1)S(1)}, bf16[128,256]{1,0:T(8,128)(2,1)}, u32[]{:S(2)}) copy-start(bf16[128,256]{1,0:T(8,128)(2,1)} %param.20) | copy-start | bytes 196612
  30.7 13.2 %all-to-all-start.1 = ((bf16[16,1,4]{2,1,0:T(2,128)(2,1)}), bf16[16,1,4]{2,1,0:T(2,128)(2,1)S(1)}, u32[]{:S(2)}, u32[]{:S(2)}) async-start(bf16[16,1,4]{2,1,0:T(2,128)(2,1)} %broadcast_in_dim.21), calls=%async_computation.1 | async-start | bytes 16384 | tf_op jit(solution)/shard_map/all_to_all | solution.py:14
  44.5 9.9 %all-to-all-start.2 = ((bf16[16,4,128]{2,1,0:T(4,128)(2,1)}), bf16[16,4,128]{2,1,0:T(4,128)(2,1)S(1)}, u32[]{:S(2)}, u32[]{:S(2)}) async-start(bf16[16,4,128]{2,1,0:T(4,128)(2,1)} %broadcast_in_dim.22), calls=%async_computation.2 | async-start | bytes 32768 | tf_op jit(solution)/shard_map/all_to_all | solution.py:14
  54.5 7.6 %copy-start.10 = (bf16[128,256]{1,0:T(8,128)(2,1)S(1)}, bf16[128,256]{1,0:T(8,128)(2,1)}, u32[]{:S(2)}) copy-start(bf16[128,256]{1,0:T(8,128)(2,1)} %param.19) | copy-start | bytes 196612
  55.1 7.8 %copy-start.6 = (bf16[128,512]{1,0:T(8,128)(2,1)S(1)}, bf16[128,512]{1,0:T(8,128)(2,1)}, u32[]{:S(2)}) copy-start(bf16[128,512]{1,0:T(8,128)(2,1)} %param.21) | copy-start | bytes 393220
  55.1 19.3 %all-to-all-start.5 = ((bf16[32,2,256]{2,1,0:T(2,128)(2,1)}), bf16[32,2,256]{2,1,0:T(2,128)(2,1)S(1)}, u32[]{:S(2)}, u32[]{:S(2)}) async-start(bf16[32,2,256]{2,1,0:T(2,128)(2,1)} %reshape.373), calls=%async_computation.5 | async-start | bytes 65536 | tf_op jit(solution)/shard_map/all_to_all | solution.py:40
  62.9 16.0 %copy-start.7 = (bf16[128,512]{1,0:T(8,128)(2,1)S(1)}, bf16[128,512]{1,0:T(8,128)(2,1)}, u32[]{:S(2)}) copy-start(bf16[128,512]{1,0:T(8,128)(2,1)} %param.22) | copy-start | bytes 393220
  74.4 16.8 %all-to-all-start.4 = ((bf16[32,2,256]{2,1,0:T(2,128)(2,1)}), bf16[32,2,256]{2,1,0:T(2,128)(2,1)S(1)}, u32[]{:S(2)}, u32[]{:S(2)}) async-start(bf16[32,2,256]{2,1,0:T(2,128)(2,1)} %reshape.372), calls=%async_computation.4 | async-start | bytes 65536 | tf_op jit(solution)/shard_map/all_to_all | solution.py:40
  79.0 16.9 %copy-start.5 = (bf16[2,1,128,256]{3,2,1,0:T(8,128)(2,1)S(1)}, bf16[2,1,128,256]{3,2,1,0:T(8,128)(2,1)}, u32[]{:S(2)}) copy-start(bf16[2,1,128,256]{3,2,1,0:T(8,128)(2,1)} %param.25) | copy-start | bytes 393220
  79.7 16.5 %copy-start.1 = (bf16[2,1,128,512]{3,2,1,0:T(8,128)(2,1)S(1)}, bf16[2,1,128,512]{3,2,1,0:T(8,128)(2,1)}, u32[]{:S(2)}) copy-start(bf16[2,1,128,512]{3,2,1,0:T(8,128)(2,1)} %param.26) | copy-start | bytes 786436
  91.1 17.6 %all-to-all-start.6 = ((bf16[32,2,512]{2,1,0:T(2,128)(2,1)}), bf16[32,2,512]{2,1,0:T(2,128)(2,1)S(1)}, u32[]{:S(2)}, u32[]{:S(2)}) async-start(bf16[32,2,512]{2,1,0:T(2,128)(2,1)} %reshape.374), calls=%async_computation.6 | async-start | bytes 131072 | tf_op jit(solution)/shard_map/all_to_all | solution.py:40
  108.7 18.2 %all-to-all-start.3 = ((bf16[32,2,512]{2,1,0:T(2,128)(2,1)}), bf16[32,2,512]{2,1,0:T(2,128)(2,1)S(1)}, u32[]{:S(2)}, u32[]{:S(2)}) async-start(bf16[32,2,512]{2,1,0:T(2,128)(2,1)} %reshape.371), calls=%async_computation.3 | async-start | bytes 131072 | tf_op jit(solution)/shard_map/all_to_all | solution.py:40
  114.3 12.6 %copy-start.12 = (f32[512]{0:T(512)S(1)}, f32[512]{0:T(512)}, u32[]{:S(2)}) copy-start(f32[512]{0:T(512)} %param.28) | copy-start | bytes 6148
  127.1 17.5 %copy-start.8 = (bf16[512,128]{1,0:T(8,128)(2,1)S(1)}, bf16[512,128]{1,0:T(8,128)(2,1)}, u32[]{:S(2)}) copy-start(bf16[512,128]{1,0:T(8,128)(2,1)} %param.29) | copy-start | bytes 393220
  144.6 42.5 %copy-start.2 = (bf16[128,704]{0,1:T(8,128)(2,1)S(1)}, bf16[128,704]{0,1:T(8,128)(2,1)}, u32[]{:S(2)}) copy-start(bf16[128,704]{0,1:T(8,128)(2,1)} %param.32) | copy-start | bytes 540676
  154.0 0.7 copy-start.11
  154.0 0.7 copy-start.13
  173.0 14.3 %copy-start.3 = (bf16[128,704]{0,1:T(8,128)(2,1)S(1)}, bf16[128,704]{0,1:T(8,128)(2,1)}, u32[]{:S(2)}) copy-start(bf16[128,704]{0,1:T(8,128)(2,1)} %param.31) | copy-start | bytes 540676
  173.0 10.0 %all-to-all-start.11 = ((bf16[16,4,128]{2,1,0:T(4,128)(2,1)}), bf16[16,4,128]{2,1,0:T(4,128)(2,1)S(1)}, u32[]{:S(2)}, u32[]{:S(2)}) async-start(bf16[16,4,128]{2,1,0:T(4,128)(2,1)} %broadcast_in_dim.27), calls=%async_computation.11 | async-start | bytes 32768 | tf_op jit(solution)/shard_map/all_to_all | solution.py:14
  183.6 9.7 %all-to-all-start.10 = ((bf16[16,1,4]{2,1,0:T(2,128)(2,1)}), bf16[16,1,4]{2,1,0:T(2,128)(2,1)S(1)}, u32[]{:S(2)}, u32[]{:S(2)}) async-start(bf16[16,1,4]{2,1,0:T(2,128)(2,1)} %broadcast_in_dim.26), calls=%async_computation.10 | async-start | bytes 16384 | tf_op jit(solution)/shard_map/all_to_all | solution.py:14
  193.3 24.8 %all-to-all-start.12 = ((bf16[32,2,1408]{2,1,0:T(2,128)(2,1)}), bf16[32,2,1408]{2,1,0:T(2,128)(2,1)S(1)}, u32[]{:S(2)}, u32[]{:S(2)}) async-start(bf16[32,2,1408]{2,1,0:T(2,128)(2,1)} %reshape.381), calls=%async_computation.12 | async-start | bytes 360448 | tf_op jit(solution)/shard_map/all_to_all | solution.py:40
  218.4 19.2 %copy-start.4 = (bf16[704,128]{1,0:T(8,128)(2,1)S(1)}, bf16[704,128]{1,0:T(8,128)(2,1)}, u32[]{:S(2)}) copy-start(bf16[704,128]{1,0:T(8,128)(2,1)} %param.33) | copy-start | bytes 540676
where the time goes:
time: 249 us; the launch traced here: 248 us
  waiting for transfers between devices  98.5 us (40%)
  blocking collectives  72.5 us (29%)
  starting transfers between devices  62.1 us (25%)
  local copies, waits for them, and re-layouts  8.04 us (3%)
  other arithmetic  3.44 us (1%)
    all_to_all x5, waiting for transfers between devices, summed_on_arrival(): parts = lax.all_to_all(split_up(value, dim, count), axis, 0, 0, tiled=True)  64.2 us
    all_to_all x3, blocking collectives, from_everyone(): return lax.all_to_all(copies, axis, split_axis=0, concat_axis=0, tiled=True)  54.1 us
    all_to_all x5, waiting for transfers between devices, from_everyone(): return lax.all_to_all(copies, axis, split_axis=0, concat_axis=0, tiled=True)  34.3 us
    all_to_all x5, starting transfers between devices, from_everyone(): return lax.all_to_all(copies, axis, split_axis=0, concat_axis=0, tiled=True)  34 us
    all_to_all x5, starting transfers between devices, summed_on_arrival(): parts = lax.all_to_all(split_up(value, dim, count), axis, 0, 0, tiled=True)  28 us
    all_to_all x2, blocking collectives, summed_on_arrival(): parts = lax.all_to_all(split_up(value, dim, count), axis, 0, 0, tiled=True)  18.4 us
  transfers between devices with their start and end apart: 10, of which 10 were waited for; matrix products, arithmetic and copies ran while one was open for 2% of the time, Pallas kernels for 0%

commit v1 on v0

v1 whole, which is shorter than its diff:
```python
import functools

import jax
import jax.numpy as jnp
import numpy as np
from jax import lax
from jax.experimental import pallas as pl
from jax.experimental.pallas import tpu as pltpu
from jax.sharding import PartitionSpec as P

D = 4096
EPS = 1e-06
KV = 16
ZS = 16
TP = 32
DK = 256
DV = 512
FU = 704
FP = 768
MSG = 1664
F32 = jnp.float32
BF16 = jnp.bfloat16
MESH = pl.DeviceIdType.MESH

PLANE = sorted(
    [(dy, dx) for dy in range(4) for dx in range(4) if (dy, dx) != (0, 0)],
    key=lambda o: -(min(o[0], 4 - o[0]) + min(o[1], 4 - o[1])),
)


def dot(a, b):
    return jnp.dot(a, b, preferred_element_type=F32)


def sin_cos(a):
    n = jnp.floor(a * np.float32(2.0 / np.pi) + 0.5)
    r = a - n * np.float32(1.5703125)
    r = r - n * np.float32(4.837512969970703125e-4)
    r = r - n * np.float32(7.549789954891882e-8)
    z = r * r
    s = r + r * z * (-1.6666654611e-1 + z * (8.3321608736e-3 - z * 1.9515295891e-4))
    c = 1.0 - 0.5 * z + z * z * (
        4.166664568298827e-2 + z * (-1.388731625493765e-3 + z * 2.443315711809948e-5)
    )
    m = n - 4.0 * jnp.floor(n * 0.25)
    odd = (m == 1.0) | (m == 3.0)
    sine = jnp.where(odd, c, s)
    cosine = jnp.where(odd, s, c)
    sine = jnp.where(m >= 2.0, -sine, sine)
    cosine = jnp.where((m == 1.0) | (m == 2.0), -cosine, cosine)
    return sine, cosine


def kernel(
    hid, mgain, wq, wk, wv, wg, decay, state, kblk, vblk, lens, ggain, wo, cgain, hg, hu, hd, freq,
    out,
    hid_v, mg_v, w1, state_v, kb_v, vb_v, gg_v, wo_v, cg_v, w2g, w2u, wd_v, fr_v, len_s, dec_s,
    sh, sl, sin_v, cos_v, wt_v, carry_v,
    xg, xs, lhs1, sib_s, sib_r, msg, rb, mx, mgat, lhs_f, psend, pr, mid3, lhs2, sib_s2, sib_r2,
    msg2, rb2, act, agat, lhs_d, hmsg, hr,
    lsem, ssa, rsa, sspair, rspair, ssb, rsb, ssc, rsc, ssd, rsd, ssf, rsf, ssg, rsg, ssh, rsh,
    far,
):
    k = lax.axis_index("kv")
    t = lax.axis_index("tp")
    z, c = t // 2, t % 2
    y, x = k // 4, k % 4

    def kv_peer(dy, dx):
        return ((y + dy) % 4) * 4 + (x + dx) % 4

    def z_peer(i):
        off = 8 - (i + 1) // 2
        sign = (i % 2) * 2 - 1
        return (z + sign * off + 16) % 16

    loads = [
        (hid, hid_v), (lens, len_s), (decay, dec_s), (freq, fr_v), (mgain, mg_v),
        (wq, w1.at[:, pl.ds(0, 256)]), (wk, w1.at[:, pl.ds(256, 256)]),
        (wv, w1.at[:, pl.ds(512, 512)]), (wg, w1.at[:, pl.ds(1024, 512)]),
        (state, state_v), (kblk, kb_v), (vblk, vb_v), (ggain, gg_v), (wo, wo_v), (cgain, cg_v),
        (hg, w2g), (hu, w2u), (hd, wd_v),
    ]
    copies = [pltpu.make_async_copy(a, b, lsem.at[i]) for i, (a, b) in enumerate(loads)]
    for cp in copies:
        cp.start()

    barrier = pltpu.get_barrier_semaphore()
    for dy, dx in PLANE:
        pl.semaphore_signal(
            barrier, inc=1, device_id={"kv": kv_peer(dy, dx), "tp": t}, device_id_type=MESH
        )

    @pl.loop(0, 16)
    def _(i):
        dz = i % 8 + 1 - (i % 8) // 4 * 9
        peer = ((z + dz + 16) % 16) * 2 + i // 8
        pl.semaphore_signal(barrier, inc=1, device_id={"kv": k, "tp": peer}, device_id_type=MESH)

    pl.semaphore_signal(
        barrier, inc=1, device_id={"kv": k, "tp": 2 * z + 1 - c}, device_id_type=MESH
    )

    for i in (1, 2, 3):
        copies[i].wait()
    row = lax.broadcasted_iota(jnp.int32, (2, 128), 0)
    slot = lax.broadcasted_iota(jnp.int32, (2, 128), 1)
    length = jnp.where(row == 0, len_s[0], len_s[1])
    sine, cosine = sin_cos(length.astype(F32) * fr_v[...])
    sin_v[...] = sine
    cos_v[...] = cosine
    filled = length & 127
    rate = dec_s[0]
    wt_v[...] = jnp.where(
        slot < filled, jnp.exp(-rate * (filled - slot).astype(F32)), jnp.zeros((2, 128), F32)
    )
    carry_v[...] = jnp.exp(-rate * (filled + 1).astype(F32))

    copies[0].wait()
    pl.semaphore_wait(barrier, 32)

    def to(src, dst, ss, rs, kv, tp):
        return pltpu.make_async_remote_copy(
            src_ref=src, dst_ref=dst, send_sem=ss, recv_sem=rs,
            device_id={"kv": kv, "tp": tp}, device_id_type=MESH,
        )

    for dy, dx in PLANE:
        p = kv_peer(dy, dx)
        to(hid_v, xg.at[k], ssa.at[p], rsa.at[k], p, t).start()
    for sg in (4, 12):
        pl.semaphore_signal(
            far, inc=1, device_id={"kv": k, "tp": ((z + sg) % 16) * 2 + c}, device_id_type=MESH
        )
    xg[k] = hid_v[...]

    copies[9].wait()
    for s in range(2):
        whole = state_v[s, 0]
        high = whole.astype(BF16)
        sh[s] = high
        sl[s] = (whole - high.astype(F32)).astype(BF16)
    for i in (4, 5, 6, 7, 8):
        copies[i].wait()

    def plane_wait(src, dst, ss, rs, recv):
        for dy, dx in PLANE:
            p = kv_peer(dy, dx)
            cp = to(src(p), dst(p), ss.at[p], rs.at[p], p, t)
            cp.wait_recv() if recv else cp.wait_send()

    plane_wait(lambda p: hid_v, lambda p: xg.at[p], ssa, rsa, True)
    for i in range(KV):
        rows = xg[i].astype(F32)
        xs[2 * i : 2 * i + 2, :] = rows[0:2]
        xs[32 + 2 * i : 34 + 2 * i, :] = rows[2:4]

    stream = xs[...]
    scaled = (stream * mg_v[...][None, :]).astype(BF16)
    lhs1[0] = scaled[0:32]
    lhs1[1] = scaled[32:64]

    def reduce_rows(product, send, recv, which, msgs, rbuf, ss, rs, first):
        send[...] = product(1 - c).astype(BF16)
        sib = 2 * z + 1 - c
        pair = to(send, recv, sspair.at[which], rspair.at[which], k, sib)
        pair.start()
        mine = product(c)
        pair.wait()
        both = mine + recv[...].astype(F32)
        for i in range(ZS):
            msgs[i] = both[2 * i : 2 * i + 2, :].astype(BF16)
        if first:
            pl.semaphore_wait(far, 2)

        @pl.loop(0, 15)
        def _(i):
            p = z_peer(i)
            to(msgs.at[p], rbuf.at[z], ss.at[p], rs.at[z], k, 2 * p + c).start()

        rbuf[z] = msgs[z]

        @pl.loop(0, 15)
        def _(i):
            p = z_peer(14 - i)
            to(msgs.at[p], rbuf.at[p], ss.at[p], rs.at[p], k, 2 * p + c).wait_recv()

        total = rbuf[0].astype(F32)
        for i in range(1, ZS):
            total = total + rbuf[i].astype(F32)
        scale = lax.rsqrt(
            jnp.sum(total[:, 1536:1664], axis=1, keepdims=True) * np.float32(1.0 / D) + EPS
        )
        return total, scale

    def sends_done(msgs, rbuf, ss, rs):
        @pl.loop(0, 15)
        def _(i):
            p = z_peer(i)
            to(msgs.at[p], rbuf.at[p], ss.at[p], rs.at[p], k, 2 * p + c).wait_send()

    def product1(i):
        left = lhs1[i]
        rows = xs[pl.ds(pl.multiple_of(i * 32, 32), 32), :]
        return jnp.concatenate([dot(left, w1[...]), rows * rows], axis=1)

    total, scale = reduce_rows(product1, sib_s, sib_r, 0, msg, rb, ssb, rsb, True)

    def rounded(v):
        return (scale * v).astype(BF16).astype(F32)

    queries, keys_new = rounded(total[:, 0:256]), rounded(total[:, 256:512])
    values_new, gates = rounded(total[:, 512:1024]), rounded(total[:, 1024:1536])
    sine, cosine = sin_v[...], cos_v[...]

    def rotate(v):
        a, b = v[:, 0:128], v[:, 128:256]
        return jnp.concatenate([a * cosine - b * sine, a * sine + b * cosine], axis=1)

    rot = rotate(queries).astype(BF16)
    rot_w = rot.astype(F32)
    fresh = rotate(keys_new) * np.float32(DK**-0.5)
    for i in (10, 11, 12):
        copies[i].wait()

    def pick(a, b):
        first = lax.broadcasted_iota(jnp.int32, a.shape, 0) == 0
        return jnp.where(first, a, b)

    scores = pick(*[
        lax.dot_general(rot, kb_v[s, 0], (((1,), (1,)), ((), ())), preferred_element_type=F32)
        for s in range(2)
    ])
    bw = (scores * wt_v[...]).astype(BF16)
    block_term = pick(*[dot(bw, vb_v[s, 0]) for s in range(2)])
    state_term = pick(*[dot(rot, sh[s]) + dot(rot, sl[s]) for s in range(2)])
    own_term = jnp.sum(rot_w * fresh, axis=1, keepdims=True) * values_new
    retained = own_term + block_term + carry_v[:, 0:1] * state_term
    centre = jnp.mean(retained, axis=1, keepdims=True)
    off = retained - centre
    spread = jnp.mean(off * off, axis=1, keepdims=True)
    normed = off * lax.rsqrt(spread + EPS)
    silu = gates / (1.0 + jnp.exp(-gates))
    mx[...] = (silu * normed * gg_v[...][None, :]).astype(BF16)

    def tp_gather(src, buf, ss, rs):
        @pl.loop(0, 15)
        def _(i):
            p = z_peer(i)
            for core in range(2):
                to(src, buf.at[t], ss.at[2 * p + core], rs.at[t], k, 2 * p + core).start()

        sib = 2 * z + 1 - c
        to(src, buf.at[t], ss.at[sib], rs.at[t], k, sib).start()
        buf[t] = src[...]

    def tp_wait(src, buf, ss, rs, recv):
        @pl.loop(1, 32)
        def _(i):
            p = (t + i) % 32
            cp = to(src, buf.at[p], ss.at[p], rs.at[p], k, p)
            cp.wait_recv() if recv else cp.wait_send()

    tp_gather(mx, mgat, ssc, rsc)
    plane_wait(lambda p: hid_v, lambda p: xg.at[p], ssa, rsa, False)
    sends_done(msg, rb, ssb, rsb)
    for i in (13, 14, 15, 16, 17):
        copies[i].wait()
    tp_wait(mx, mgat, ssc, rsc, True)
    for i in range(TP):
        r = 32 * (i % 2) + 2 * (i // 2)
        lhs_f[r : r + 2, :] = mgat[i].astype(F32)

    psend[...] = dot(lhs_f[...].astype(BF16), wo_v[...]).astype(BF16)
    for dy, dx in PLANE:
        p = kv_peer(dy, dx)
        to(psend, pr.at[k], ssd.at[p], rsd.at[k], p, t).start()
    pr[k] = psend[...]
    tp_wait(mx, mgat, ssc, rsc, False)
    plane_wait(lambda p: psend, lambda p: pr.at[p], ssd, rsd, True)
    middle = xs[...] + jnp.sum(pr[...].astype(F32), axis=0)
    xs[...] = middle
    scaled = (middle * cg_v[...][None, :]).astype(BF16)
    lhs2[0] = scaled[0:32]
    lhs2[1] = scaled[32:64]
    for i in range(KV):
        mid3[i, 0:2, :] = middle[2 * i : 2 * i + 2]
        mid3[i, 2:4, :] = middle[32 + 2 * i : 34 + 2 * i]

    def product2(i):
        left = lhs2[i]
        rows = xs[pl.ds(pl.multiple_of(i * 32, 32), 32), :]
        pad = jnp.zeros((32, FP - FU), F32)
        return jnp.concatenate(
            [dot(left, w2g[...]), pad, dot(left, w2u[...]), pad, rows * rows], axis=1
        )

    total, scale = reduce_rows(product2, sib_s2, sib_r2, 1, msg2, rb2, ssf, rsf, False)
    gate_part, up_part = scale * total[:, 0:FU], scale * total[:, FP : FP + FU]
    act[...] = (gate_part / (1.0 + jnp.exp(-gate_part)) * up_part).astype(BF16)
    tp_gather(act, agat, ssg, rsg)
    plane_wait(lambda p: psend, lambda p: pr.at[p], ssd, rsd, False)
    sends_done(msg2, rb2, ssf, rsf)
    tp_wait(act, agat, ssg, rsg, True)
    for i in range(TP):
        lhs_d[2 * i : 2 * i + 2, :] = agat[i].astype(F32)

    part = dot(lhs_d[...].astype(BF16), wd_v[...])
    for i in range(KV):
        hmsg[i] = part[4 * i : 4 * i + 4, :].astype(BF16)
    for dy, dx in PLANE:
        p = kv_peer(dy, dx)
        to(hmsg.at[p], hr.at[k], ssh.at[p], rsh.at[k], p, t).start()
    hr[k] = hmsg[k]
    tp_wait(act, agat, ssg, rsg, False)
    plane_wait(lambda p: hmsg.at[p], lambda p: hr.at[p], ssh, rsh, True)
    out[...] = (mid3[k] + jnp.sum(hr[...].astype(F32), axis=0)).astype(BF16)
    plane_wait(lambda p: hmsg.at[p], lambda p: hr.at[p], ssh, rsh, False)


def scratch():
    v = pltpu.VMEM
    dma = pltpu.SemaphoreType.DMA
    return [
        v((4, 128), BF16), v((128,), F32), v((128, 1536), BF16), v((2, 1, 256, 512), F32),
        v((2, 1, 128, 256), BF16), v((2, 1, 128, 512), BF16), v((512,), F32), v((512, 128), BF16),
        v((128,), F32), v((128, FU), BF16), v((128, FU), BF16), v((FU, 128), BF16),
        v((1, 128), F32), pltpu.SMEM((2,), jnp.int32), pltpu.SMEM((1,), F32),
        v((2, 256, 512), BF16), v((2, 256, 512), BF16),
        v((2, 128), F32), v((2, 128), F32), v((2, 128), F32), v((2, 128), F32),
        v((KV, 4, 128), BF16), v((64, 128), F32), v((2, 32, 128), BF16),
        v((32, MSG), BF16), v((32, MSG), BF16), v((ZS, 2, MSG), BF16), v((ZS, 2, MSG), BF16),
        v((2, DV), BF16), v((TP, 2, DV), BF16), v((64, DV), F32),
        v((64, 128), BF16), v((KV, 64, 128), BF16), v((KV, 4, 128), F32), v((2, 32, 128), BF16),
        v((32, MSG), BF16), v((32, MSG), BF16), v((ZS, 2, MSG), BF16), v((ZS, 2, MSG), BF16),
        v((2, FU), BF16), v((TP, 2, FU), BF16), v((64, FU), F32),
        v((KV, 4, 128), BF16), v((KV, 4, 128), BF16),
        dma((18,)), dma((KV,)), dma((KV,)), dma((2,)), dma((2,)), dma((ZS,)), dma((ZS,)),
        dma((TP,)), dma((TP,)), dma((KV,)), dma((KV,)), dma((ZS,)), dma((ZS,)),
        dma((TP,)), dma((TP,)), dma((KV,)), dma((KV,)),
        pltpu.SemaphoreType.REGULAR,
    ]


def local(*args):
    freq = jnp.asarray(
        (10000.0 ** (-np.arange(128, dtype=np.float64) / 128)).astype(np.float32)[None, :]
    )
    return pl.pallas_call(
        kernel,
        out_shape=jax.ShapeDtypeStruct((4, 128), BF16),
        in_specs=[pl.BlockSpec(memory_space=pl.ANY)] * 18,
        out_specs=pl.BlockSpec(memory_space=pltpu.VMEM),
        scratch_shapes=scratch(),
        compiler_params=pltpu.CompilerParams(
            collective_id=0, has_side_effects=True, vmem_limit_bytes=48 * 1024 * 1024
        ),
    )(*args, freq)


def solution(mesh):
    in_specs = (
        P("kv", "tp"), P("tp"), P("tp", "kv"), P("tp", "kv"), P("tp", "kv"), P("tp", "kv"),
        P("kv"), P("tp", "kv", None, None), P("tp", "kv", None, None), P("tp", "kv", None, None),
        P("tp"), P("kv"), P("kv", "tp"), P("tp"), P("tp", "kv"), P("tp", "kv"), P("kv", "tp"),
    )
    return jax.shard_map(
        local, mesh=mesh, in_specs=in_specs, out_specs=P("kv", "tp"), check_vma=False
    )
```

time: 249 us -> 78.1 us (0.31)
  waiting for transfers between devices: 98.5 us -> 0 us
  blocking collectives: 72.5 us -> 0 us
  Pallas kernels: 0 us -> 69.4 us
  starting transfers between devices: 62.1 us -> 0 us
  other arithmetic: 3.44 us -> 0 us
    all_to_all x10 -> x0, waiting for transfers between devices: 98.5 us -> none  [the longest x5 64.2 us: summed_on_arrival(): parts = lax.all_to_all(split_up(value, dim, count), axis, 0, 0, tiled=True)]
    all_to_all x5 -> x0, blocking collectives: 72.5 us -> none  [the longest x3 54.1 us: from_everyone(): return lax.all_to_all(copies, axis, split_axis=0, concat_axis=0, tiled=True)]
    pallas_call x0 -> x1, Pallas kernels: none -> 69.4 us  [local(): pl.pallas_call(kernel, out_shape=jax.ShapeDtypeStruct((4, 128), BF16), in...]
    all_to_all x10 -> x0, starting transfers between devices: 62.1 us -> none  [the longest x5 34 us: from_everyone(): return lax.all_to_all(copies, axis, split_axis=0, concat_axis=0, tiled=True)]
    unnamed x30 -> x33, local copies, waits for them, and re-layouts: 1.36 us -> 7.58 us
    reshape x7 -> x0, local copies, waits for them, and re-layouts: 3.39 us -> none  [the longest x5 3.3 us: split_up(): value.reshape(*shape[:dim], count, shape[dim] // count, *shape[dim + 1:])]
    broadcast_in_dim x8 -> x0, local copies, waits for them, and re-layouts: 3.12 us -> none  [from_everyone(): copies = jnp.broadcast_to(value, (lax.axis_size(axis), *value.shape))]
  transfers between devices with their start and end apart: 10 -> 0, of which waited for: 10 -> 0; matrix products, arithmetic and copies ran while one was open for 2% -> 0% of each run, Pallas kernels for 0% -> 0%
where the time goes in v1:
time: 78.1 us; the launch traced here: 77.8 us
  Pallas kernels  69.4 us (89%)
  local copies, waits for them, and re-layouts  7.58 us (10%)
  between operations  0.84 us (1%)
    pallas_call x1, Pallas kernels, local(): pl.pallas_call(kernel, out_shape=jax.ShapeDtypeStruct((4, 128), BF16), in...  69.4 us
    unnamed x33, local copies, waits for them, and re-layouts  7.58 us

profile of v1, /device:TPU:1, one launch (start us, length us, event | category | flops | bytes accessed | tf_op | source)
XLA Modules:
  0.0 77.8 jit_solution(16976282375034846931)
XLA Ops:
  0.7 0.0 copy-start.2
  0.7 0.0 copy-start.3
  0.7 0.0 copy-start.4
  0.7 1.1 %copy.19.hg = bf16[128,704]{1,0:T(8,128)(2,1)S(1)} copy(bf16[128,704]{0,1:T(8,128)(2,1)} %param.32) | data formatting | bytes 360448 | tf_op args[14]
  1.8 0.0 copy-start.1
  1.8 0.0 copy-start.9
  1.8 0.0 copy-start.10
  1.8 0.0 copy-start.11
  1.8 0.0 copy-start.12
  1.9 0.0 copy-start.13
  1.9 0.0 copy-start.14
  1.9 1.1 %copy.20.hu = bf16[128,704]{1,0:T(8,128)(2,1)S(1)} copy(bf16[128,704]{0,1:T(8,128)(2,1)} %param.33) | data formatting | bytes 360448 | tf_op args[15]
  3.0 0.0 copy-done.2
  3.0 0.0 copy-done.3
  3.0 0.0 copy-done.4
  3.1 0.0 copy-done.1
  3.1 0.0 copy-done.9
  3.1 0.0 copy-done.10
  3.1 0.0 copy-done.11
  3.1 0.0 copy-done.12
  3.1 0.0 copy-done.13
  3.1 0.0 copy-done.14
  3.1 0.0 copy-start
  3.1 1.2 %copy-done = f32[2,1,256,512]{3,2,1,0:T(8,128)S(1)} copy-done((f32[2,1,256,512]{3,2,1,0:T(8,128)S(1)}, f32[2,1,256,512]{3,2,1,0:T(8,128)}, u32[]{:S(2)}) %copy-start) | copy-done | bytes 1048600
  4.4 0.0 copy-start.5
  4.4 0.9 %copy-done.5 = bf16[2,1,128,256]{3,2,1,0:T(8,128)(2,1)S(1)} copy-done((bf16[2,1,128,256]{3,2,1,0:T(8,128)(2,1)S(1)}, bf16[2,1,128,256]{3,2,1,0:T(8,128)(2,1)}, u32[]{:S(2)}) %copy-start.5) | copy-done | bytes 131096
  5.3 0.0 copy-start.6
  5.3 0.9 %copy-done.6 = bf16[512,128]{1,0:T(8,128)(2,1)S(1)} copy-done((bf16[512,128]{1,0:T(8,128)(2,1)S(1)}, bf16[512,128]{1,0:T(8,128)(2,1)}, u32[]{:S(2)}) %copy-start.6) | copy-done | bytes 131096
  6.2 0.0 copy-start.7
  6.2 0.8 %copy-done.7 = bf16[128,256]{1,0:T(8,128)(2,1)S(1)} copy-done((bf16[128,256]{1,0:T(8,128)(2,1)S(1)}, bf16[128,256]{1,0:T(8,128)(2,1)}, u32[]{:S(2)}) %copy-start.7) | copy-done | bytes 65560
  7.0 0.0 copy-start.8
  7.0 0.8 %copy-done.8 = bf16[128,256]{1,0:T(8,128)(2,1)S(1)} copy-done((bf16[128,256]{1,0:T(8,128)(2,1)S(1)}, bf16[128,256]{1,0:T(8,128)(2,1)}, u32[]{:S(2)}) %copy-start.8) | copy-done | bytes 65560
  7.8 69.4 %shard_map.172 = bf16[4,128]{1,0:T(4,128)(2,1)S(1)} custom-call(bf16[4,128]{1,0:T(4,128)(2,1)S(1)} %copy-done.10, f32[128]{0:T(128)S(1)} %copy-done.11, bf16[128,256]{1,0:T(8,128)(2,1)S(1)} %copy-done.7, bf16[128,256]{1,0:T(8,128)(2,1)S(1)} %copy-done.8, bf16[128,512]{1,0:T(8,128)(2,1)S(1)} %copy-done.3, bf16[128,512]{1,0:T(8,128)(2,1)S(1)} %copy-done.4, ...), custom_call_target="tpu_custom_call" | custom-call | tf_op jit(solution)/shard_map/pallas_call | solution.py:349
  77.3 0.6 copy.23
Async XLA Ops:
  0.7 2.4 %copy-start.2 = (bf16[704,128]{1,0:T(8,128)(2,1)S(1)}, bf16[704,128]{1,0:T(8,128)(2,1)}, u32[]{:S(2)}) copy-start(bf16[704,128]{1,0:T(8,128)(2,1)} %hd.1) | copy-start | bytes 540676
  0.7 2.4 %copy-start.3 = (bf16[128,512]{1,0:T(8,128)(2,1)S(1)}, bf16[128,512]{1,0:T(8,128)(2,1)}, u32[]{:S(2)}) copy-start(bf16[128,512]{1,0:T(8,128)(2,1)} %wv.1) | copy-start | bytes 393220
  0.7 2.4 %copy-start.4 = (bf16[128,512]{1,0:T(8,128)(2,1)S(1)}, bf16[128,512]{1,0:T(8,128)(2,1)}, u32[]{:S(2)}) copy-start(bf16[128,512]{1,0:T(8,128)(2,1)} %wg.1) | copy-start | bytes 393220
  1.8 1.3 %copy-start.1 = (bf16[2,1,128,512]{3,2,1,0:T(8,128)(2,1)S(1)}, bf16[2,1,128,512]{3,2,1,0:T(8,128)(2,1)}, u32[]{:S(2)}) copy-start(bf16[2,1,128,512]{3,2,1,0:T(8,128)(2,1)} %vblk.1) | copy-start | bytes 786436
  1.8 1.3 %copy-start.9 = (f32[512]{0:T(512)S(1)}, f32[512]{0:T(512)}, u32[]{:S(2)}) copy-start(f32[512]{0:T(512)} %ggain.1) | copy-start | bytes 6148
  1.8 1.3 %copy-start.10 = (bf16[4,128]{1,0:T(4,128)(2,1)S(1)}, bf16[4,128]{1,0:T(4,128)(2,1)}, u32[]{:S(2)}) copy-start(bf16[4,128]{1,0:T(4,128)(2,1)} %hid.1) | copy-start | bytes 3076
  1.8 1.3 %copy-start.11 = (f32[128]{0:T(128)S(1)}, f32[128]{0:T(128)}, u32[]{:S(2)}) copy-start(f32[128]{0:T(128)} %mgain.1) | copy-start | bytes 1540
  1.8 1.3 %copy-start.12 = (s32[2]{0:T(128)S(1)}, s32[2]{0:T(128)}, u32[]{:S(2)}) copy-start(s32[2]{0:T(128)} %lens.1) | copy-start | bytes 28
  1.9 1.3 %copy-start.13 = (f32[128]{0:T(128)S(1)}, f32[128]{0:T(128)}, u32[]{:S(2)}) copy-start(f32[128]{0:T(128)} %cgain.1) | copy-start | bytes 1540
  1.9 1.3 %copy-start.14 = (f32[1,128]{1,0:T(1,128)S(1)}, f32[1,128]{1,0:T(1,128)}, u32[]{:S(2)}) copy-start(f32[1,128]{1,0:T(1,128)} %constant.2.clone.freq) | copy-start | bytes 1540
  3.1 1.2 %copy-start = (f32[2,1,256,512]{3,2,1,0:T(8,128)S(1)}, f32[2,1,256,512]{3,2,1,0:T(8,128)}, u32[]{:S(2)}) copy-start(f32[2,1,256,512]{3,2,1,0:T(8,128)} %state.1) | copy-start | bytes 3145732
  4.4 0.9 %copy-start.5 = (bf16[2,1,128,256]{3,2,1,0:T(8,128)(2,1)S(1)}, bf16[2,1,128,256]{3,2,1,0:T(8,128)(2,1)}, u32[]{:S(2)}) copy-start(bf16[2,1,128,256]{3,2,1,0:T(8,128)(2,1)} %kblk.1) | copy-start | bytes 393220
  5.3 0.9 %copy-start.6 = (bf16[512,128]{1,0:T(8,128)(2,1)S(1)}, bf16[512,128]{1,0:T(8,128)(2,1)}, u32[]{:S(2)}) copy-start(bf16[512,128]{1,0:T(8,128)(2,1)} %wo.1) | copy-start | bytes 393220
  6.2 0.8 %copy-start.7 = (bf16[128,256]{1,0:T(8,128)(2,1)S(1)}, bf16[128,256]{1,0:T(8,128)(2,1)}, u32[]{:S(2)}) copy-start(bf16[128,256]{1,0:T(8,128)(2,1)} %wq.1) | copy-start | bytes 196612
  7.0 0.8 %copy-start.8 = (bf16[128,256]{1,0:T(8,128)(2,1)S(1)}, bf16[128,256]{1,0:T(8,128)(2,1)}, u32[]{:S(2)}) copy-start(bf16[128,256]{1,0:T(8,128)(2,1)} %wk.1) | copy-start | bytes 196612

commit v2 on v1

v2 whole, which is shorter than its diff:
```python
import functools

import jax
import jax.numpy as jnp
import numpy as np
from jax import lax
from jax.experimental import pallas as pl
from jax.experimental.pallas import tpu as pltpu
from jax.sharding import PartitionSpec as P

D = 4096
EPS = 1e-06
KV = 16
ZS = 16
TP = 32
DK = 256
DV = 512
FU = 704
FP = 768
MSG = 1664
UPTO = 99
F32 = jnp.float32
BF16 = jnp.bfloat16
MESH = pl.DeviceIdType.MESH

PLANE = sorted(
    [(dy, dx) for dy in range(4) for dx in range(4) if (dy, dx) != (0, 0)],
    key=lambda o: -(min(o[0], 4 - o[0]) + min(o[1], 4 - o[1])),
)


def dot(a, b):
    return jnp.dot(a, b, preferred_element_type=F32)


def dot_t(a, b):
    return lax.dot_general(a, b, (((1,), (1,)), ((), ())), preferred_element_type=F32)


def sin_cos(a):
    n = jnp.floor(a * np.float32(2.0 / np.pi) + 0.5)
    r = a - n * np.float32(1.5703125)
    r = r - n * np.float32(4.837512969970703125e-4)
    r = r - n * np.float32(7.549789954891882e-8)
    z = r * r
    s = r + r * z * (-1.6666654611e-1 + z * (8.3321608736e-3 - z * 1.9515295891e-4))
    c = 1.0 - 0.5 * z + z * z * (
        4.166664568298827e-2 + z * (-1.388731625493765e-3 + z * 2.443315711809948e-5)
    )
    m = n - 4.0 * jnp.floor(n * 0.25)
    odd = (m == 1.0) | (m == 3.0)
    sine = jnp.where(odd, c, s)
    cosine = jnp.where(odd, s, c)
    sine = jnp.where(m >= 2.0, -sine, sine)
    cosine = jnp.where((m == 1.0) | (m == 2.0), -cosine, cosine)
    return sine, cosine


def kernel(
    hid, mgain, wq, wk, wv, wg, decay, state, kblk, vblk, lens, ggain, wo, cgain, hg, hu, hd, freq,
    out,
    hid_v, mg_v, w1, state_v, kb_v, vb_v, gg_v, wo_v, cg_v, w2g, w2u, wd_v, fr_v, len_s, dec_s,
    sh, sl, sin_v, cos_v, wt_v, carry_v,
    xg, xs, lhs1, sib_s, sib_r, msg, rb, mx, mgat, lhs_f, psend, pr, mid3, lhs2, sib_s2, sib_r2,
    msg2, rb2, act, agat, lhs_d, hmsg, hr,
    lsem, ssa, rsa, sspair, rspair, ssb, rsb, ssc, rsc, ssd, rsd, ssf, rsf, ssg, rsg, ssh, rsh,
    far,
):
    k = lax.axis_index("kv")
    t = lax.axis_index("tp")
    z, c = t // 2, t % 2
    y, x = k // 4, k % 4
    sib = 2 * z + 1 - c
    pending = []

    def kv_peer(dy, dx):
        return ((y + dy) % 4) * 4 + (x + dx) % 4

    def z_peer(i):
        off = 8 - (i + 1) // 2
        sign = (i % 2) * 2 - 1
        return (z + sign * off + 16) % 16

    def drain(n=None):
        for _ in range(len(pending) if n is None else n):
            pending.pop(0)()

    def to(src, dst, ss, rs, kv, tp):
        return pltpu.make_async_remote_copy(
            src_ref=src, dst_ref=dst, send_sem=ss, recv_sem=rs,
            device_id={"kv": kv, "tp": tp}, device_id_type=MESH,
        )

    def signal(sem, kv, tp):
        pl.semaphore_signal(sem, inc=1, device_id={"kv": kv, "tp": tp}, device_id_type=MESH)

    loads = [
        (hid, hid_v), (lens, len_s), (decay, dec_s), (freq, fr_v), (mgain, mg_v),
        (wq, w1.at[:, pl.ds(0, 256)]), (wk, w1.at[:, pl.ds(256, 256)]),
        (wv, w1.at[:, pl.ds(512, 512)]), (wg, w1.at[:, pl.ds(1024, 512)]),
        (state, state_v), (kblk, kb_v), (vblk, vb_v), (ggain, gg_v), (wo, wo_v), (cgain, cg_v),
        (hg, w2g), (hu, w2u), (hd, wd_v),
    ]
    copies = [pltpu.make_async_copy(a, b, lsem.at[i]) for i, (a, b) in enumerate(loads)]
    loaded = [0] * len(loads)

    def need(*ids):
        for i in ids:
            if not loaded[i]:
                copies[i].wait()
                loaded[i] = 1

    barrier = pltpu.get_barrier_semaphore()
    for dy, dx in PLANE:
        signal(barrier, kv_peer(dy, dx), t)
    copies[0].start()

    @pl.loop(0, 16)
    def _(i):
        dz = 4 - (i % 8) // 2
        dz = dz - 2 * dz * (i % 2)
        signal(barrier, k, ((z + dz + 16) % 16) * 2 + i // 8)

    signal(barrier, k, sib)
    for cp in copies[1:]:
        cp.start()

    need(1, 2, 3)
    row = lax.broadcasted_iota(jnp.int32, (2, 128), 0)
    slot = lax.broadcasted_iota(jnp.int32, (2, 128), 1)
    length = jnp.where(row == 0, len_s[0], len_s[1])
    sine, cosine = sin_cos(length.astype(F32) * fr_v[...])
    sin_v[...] = sine
    cos_v[...] = cosine
    filled = length & 127
    rate = dec_s[0]
    wt_v[...] = jnp.where(
        slot < filled, jnp.exp(-rate * (filled - slot).astype(F32)), jnp.zeros((2, 128), F32)
    )
    carry_v[...] = jnp.exp(-rate * (filled + 1).astype(F32))

    need(0)
    pl.semaphore_wait(barrier, 32)

    def stop(value):
        drain()
        need(*range(len(loads)))
        out[...] = jnp.broadcast_to(value, (4, 128)).astype(BF16)

    for sg in (4, 12):
        signal(far, k, ((z + sg) % 16) * 2 + c)
    if UPTO == 0:
        pl.semaphore_wait(far, 2)
        return stop(sin_v[0:1, :])

    def plane_start(src, dst, ss, rs):
        for dy, dx in PLANE:
            p = kv_peer(dy, dx)
            to(src(p), dst.at[k], ss, rs, p, t).start()
        pending.append(lambda: all_done(dst, KV - 1, ss))

    def all_done(buf, n, sem):
        part = buf.at[pl.ds(0, n)]
        pltpu.make_async_copy(part, part, sem).wait()

    plane_start(lambda p: hid_v, xg, ssa, rsa)
    xg[k] = hid_v[...]

    need(9)
    for s in range(2):
        whole = state_v[s, 0]
        high = whole.astype(BF16)
        sh[s] = high
        sl[s] = (whole - high.astype(F32)).astype(BF16)
    need(4, 5, 6, 7, 8)

    all_done(xg, KV - 1, rsa)
    for i in range(KV):
        rows = xg[i].astype(F32)
        xs[2 * i : 2 * i + 2, :] = rows[0:2]
        xs[32 + 2 * i : 34 + 2 * i, :] = rows[2:4]
    if UPTO == 1:
        pl.semaphore_wait(far, 2)
        return stop(xs[0:4, :])

    stream = xs[...]
    scaled = (stream * mg_v[...][None, :]).astype(BF16)
    lhs1[0] = scaled[0:32]
    lhs1[1] = scaled[32:64]

    def pair_sum(product, send, recv, which, msgs):
        def lay_out(rows, dst):
            for i in range(ZS):
                dst[i] = rows[2 * i : 2 * i + 2, :].astype(BF16)

        lay_out(product(1 - c), send)
        pair = to(send, recv, sspair.at[which], rspair.at[which], k, sib)
        pair.start()
        lay_out(product(c), msgs)
        pair.wait()
        msgs[...] = msgs[...] + recv[...]

    def z_scatter(msgs, rbuf, ss, rs):
        @pl.loop(0, 15)
        def _(i):
            p = z_peer(i)
            to(msgs.at[p], rbuf.at[z], ss, rs, k, 2 * p + c).start()

        rbuf[z] = msgs[z]
        pending.append(lambda: all_done(rbuf, ZS - 1, ss))
        all_done(rbuf, ZS - 1, rs)

    def z_total(rbuf):
        total = rbuf[0].astype(F32)
        for i in range(1, ZS):
            total = total + rbuf[i].astype(F32)
        scale = lax.rsqrt(
            jnp.sum(total[:, 1536:1664], axis=1, keepdims=True) * np.float32(1.0 / D) + EPS
        )
        return total, scale

    def product1(i):
        left = lhs1[i]
        rows = xs[pl.ds(pl.multiple_of(i * 32, 32), 32), :]
        return jnp.concatenate([dot(left, w1[...]), rows * rows], axis=1)

    pair_sum(product1, sib_s, sib_r, 0, msg)
    pl.semaphore_wait(far, 2)
    if UPTO == 2:
        return stop(msg[0, :, 0:128].astype(F32)[0:1, :])
    z_scatter(msg, rb, ssb, rsb)
    if UPTO == 3:
        return stop(rb[0, :, 0:128].astype(F32)[0:1, :])
    total, scale = z_total(rb)

    def rounded(v):
        return (scale * v).astype(BF16).astype(F32)

    queries, keys_new = rounded(total[:, 0:256]), rounded(total[:, 256:512])
    values_new, gates = rounded(total[:, 512:1024]), rounded(total[:, 1024:1536])
    sine, cosine = sin_v[...], cos_v[...]

    def rotate(v):
        a, b = v[:, 0:128], v[:, 128:256]
        return jnp.concatenate([a * cosine - b * sine, a * sine + b * cosine], axis=1)

    rot = rotate(queries).astype(BF16)
    rot_w = rot.astype(F32)
    fresh = rotate(keys_new) * np.float32(DK**-0.5)
    need(10, 11, 12)

    def pick(a, b):
        first = lax.broadcasted_iota(jnp.int32, a.shape, 0) == 0
        return jnp.where(first, a, b)

    scores = pick(*[dot_t(rot, kb_v[s, 0]) for s in range(2)])
    bw = (scores * wt_v[...]).astype(BF16)
    block_term = pick(*[dot(bw, vb_v[s, 0]) for s in range(2)])
    state_term = pick(*[dot(rot, sh[s]) + dot(rot, sl[s]) for s in range(2)])
    own_term = jnp.sum(rot_w * fresh, axis=1, keepdims=True) * values_new
    retained = own_term + block_term + carry_v[:, 0:1] * state_term
    centre = jnp.mean(retained, axis=1, keepdims=True)
    off = retained - centre
    spread = jnp.mean(off * off, axis=1, keepdims=True)
    normed = off * lax.rsqrt(spread + EPS)
    silu = gates / (1.0 + jnp.exp(-gates))
    mx[...] = (silu * normed * gg_v[...][None, :]).astype(BF16)
    if UPTO == 4:
        return stop(mx[:, 0:128].astype(F32)[0:1, :])

    def tp_start(src, buf, ss, rs):
        @pl.loop(0, 15)
        def _(i):
            p = z_peer(i)
            for core in range(2):
                to(src, buf.at[t], ss, rs, k, 2 * p + core).start()

        to(src, buf.at[t], ss, rs, k, sib).start()
        buf[t] = src[...]
        pending.append(lambda: all_done(buf, TP - 1, ss))

    tp_start(mx, mgat, ssc, rsc)
    drain(2)
    need(13, 14, 15, 16, 17)
    all_done(mgat, TP - 1, rsc)
    if UPTO == 5:
        return stop(mgat[0, :, 0:128].astype(F32)[0:1, :])
    for i in range(TP):
        r = 32 * (i % 2) + 2 * (i // 2)
        lhs_f[r : r + 2, :] = mgat[i].astype(F32)

    psend[...] = dot(lhs_f[...].astype(BF16), wo_v[...]).astype(BF16)
    if UPTO == 6:
        return stop(psend[0:16, :].astype(F32)[0:1, :])
    plane_start(lambda p: psend, pr, ssd, rsd)
    pr[k] = psend[...]
    drain(1)
    all_done(pr, KV - 1, rsd)
    if UPTO == 7:
        return stop(pr[0, 0:16, :].astype(F32)[0:1, :])
    middle = xs[...] + jnp.sum(pr[...].astype(F32), axis=0)
    xs[...] = middle
    scaled = (middle * cg_v[...][None, :]).astype(BF16)
    lhs2[0] = scaled[0:32]
    lhs2[1] = scaled[32:64]
    for i in range(KV):
        mid3[i, 0:2, :] = middle[2 * i : 2 * i + 2]
        mid3[i, 2:4, :] = middle[32 + 2 * i : 34 + 2 * i]

    def product2(i):
        left = lhs2[i]
        rows = xs[pl.ds(pl.multiple_of(i * 32, 32), 32), :]
        pad = jnp.zeros((32, FP - FU), F32)
        return jnp.concatenate(
            [dot_t(left, w2g[...]), pad, dot_t(left, w2u[...]), pad, rows * rows], axis=1
        )

    pair_sum(product2, sib_s2, sib_r2, 1, msg2)
    if UPTO == 8:
        return stop(msg2[0, :, 0:128].astype(F32)[0:1, :])
    z_scatter(msg2, rb2, ssf, rsf)
    total, scale = z_total(rb2)
    gate_part, up_part = scale * total[:, 0:FU], scale * total[:, FP : FP + FU]
    act[...] = (gate_part / (1.0 + jnp.exp(-gate_part)) * up_part).astype(BF16)
    if UPTO == 9:
        return stop(act[:, 0:128].astype(F32)[0:1, :])
    tp_start(act, agat, ssg, rsg)
    drain(2)
    all_done(agat, TP - 1, rsg)
    if UPTO == 10:
        return stop(agat[0, :, 0:128].astype(F32)[0:1, :])
    for i in range(TP):
        lhs_d[2 * i : 2 * i + 2, :] = agat[i].astype(F32)

    part = dot(lhs_d[...].astype(BF16), wd_v[...])
    for i in range(KV):
        hmsg[i] = part[4 * i : 4 * i + 4, :].astype(BF16)
    if UPTO == 11:
        return stop(hmsg[0].astype(F32))
    plane_start(lambda p: hmsg.at[p], hr, ssh, rsh)
    hr[k] = hmsg[k]
    drain(1)
    all_done(hr, KV - 1, rsh)
    out[...] = (mid3[k] + jnp.sum(hr[...].astype(F32), axis=0)).astype(BF16)
    drain()


def scratch():
    v = pltpu.VMEM
    dma = pltpu.SemaphoreType.DMA
    return [
        v((4, 128), BF16), v((128,), F32), v((128, 1536), BF16), v((2, 1, 256, 512), F32),
        v((2, 1, 128, 256), BF16), v((2, 1, 128, 512), BF16), v((512,), F32), v((512, 128), BF16),
        v((128,), F32), v((FU, 128), BF16), v((FU, 128), BF16), v((FU, 128), BF16),
        v((1, 128), F32), pltpu.SMEM((2,), jnp.int32), pltpu.SMEM((1,), F32),
        v((2, 256, 512), BF16), v((2, 256, 512), BF16),
        v((2, 128), F32), v((2, 128), F32), v((2, 128), F32), v((2, 128), F32),
        v((KV, 4, 128), BF16), v((64, 128), F32), v((2, 32, 128), BF16),
        v((ZS, 2, MSG), BF16), v((ZS, 2, MSG), BF16), v((ZS, 2, MSG), BF16), v((ZS, 2, MSG), BF16),
        v((2, DV), BF16), v((TP, 2, DV), BF16), v((64, DV), F32),
        v((64, 128), BF16), v((KV, 64, 128), BF16), v((KV, 4, 128), F32), v((2, 32, 128), BF16),
        v((ZS, 2, MSG), BF16), v((ZS, 2, MSG), BF16), v((ZS, 2, MSG), BF16), v((ZS, 2, MSG), BF16),
        v((2, FU), BF16), v((TP, 2, FU), BF16), v((64, FU), F32),
        v((KV, 4, 128), BF16), v((KV, 4, 128), BF16),
        dma((18,)), dma, dma, dma((2,)), dma((2,)), *[dma] * 12,
        pltpu.SemaphoreType.REGULAR,
    ]


def local(*args):
    freq = jnp.asarray(
        (10000.0 ** (-np.arange(128, dtype=np.float64) / 128)).astype(np.float32)[None, :]
    )
    args = (*args[:14], args[14].T, args[15].T, args[16])
    return pl.pallas_call(
        kernel,
        out_shape=jax.ShapeDtypeStruct((4, 128), BF16),
        in_specs=[pl.BlockSpec(memory_space=pltpu.HBM)] * 18,
        out_specs=pl.BlockSpec(memory_space=pltpu.VMEM),
        scratch_shapes=scratch(),
        compiler_params=pltpu.CompilerParams(
            collective_id=0, has_side_effects=True, vmem_limit_bytes=58000000
        ),
    )(*args, freq)


def solution(mesh):
    in_specs = (
        P("kv", "tp"), P("tp"), P("tp", "kv"), P("tp", "kv"), P("tp", "kv"), P("tp", "kv"),
        P("kv"), P("tp", "kv", None, None), P("tp", "kv", None, None), P("tp", "kv", None, None),
        P("tp"), P("kv"), P("kv", "tp"), P("tp"), P("tp", "kv"), P("tp", "kv"), P("kv", "tp"),
    )
    return jax.shard_map(
        local, mesh=mesh, in_specs=in_specs, out_specs=P("kv", "tp"), check_vma=False
    )
```

time: 78.1 us -> 68.1 us (0.87)
  local copies, waits for them, and re-layouts: 7.58 us -> 1.24 us
  Pallas kernels: 69.4 us -> 66 us
    unnamed x33 -> x1, local copies, waits for them, and re-layouts: 7.58 us -> 1.24 us
    pallas_call x1, Pallas kernels: 69.4 us -> 66 us  [local(): pl.pallas_call(kernel, out_shape=jax.ShapeDtypeStruct((4, 128), BF16), in...]
where the time goes in v2:
time: 68.1 us; the launch traced here: 67.9 us
  Pallas kernels  66 us (97%)
  local copies, waits for them, and re-layouts  1.24 us (2%)
    pallas_call x1, Pallas kernels, local(): pl.pallas_call(kernel, out_shape=jax.ShapeDtypeStruct((4, 128), BF16), in...  66 us

profile of v2, /device:TPU:1, one launch (start us, length us, event | category | flops | bytes accessed | tf_op | source)
XLA Modules:
  0.0 67.9 jit_solution(17913936094020863070)
XLA Ops:
  0.7 66.0 %shard_map.172 = bf16[4,128]{1,0:T(4,128)(2,1)} custom-call(bf16[4,128]{1,0:T(4,128)(2,1)} %hid.1, f32[128]{0:T(128)} %mgain.1, bf16[128,256]{1,0:T(8,128)(2,1)} %wq.1, bf16[128,256]{1,0:T(8,128)(2,1)} %wk.1, bf16[128,512]{1,0:T(8,128)(2,1)} %wv.1, bf16[128,512]{1,0:T(8,128)(2,1)} %wg.1, f32[1]{0:T(128)S(6)} %copy.20.decay, f32[2,1,256,512]{3,2,1,0:T(8,128)} %state.1, ...), custom_call_target="tpu_custom_call" | custom-call | tf_op jit(solution)/shard_map/pallas_call | solution.py:375
  66.7 1.2 %copy.21 = bf16[4,128]{1,0:T(4,128)(2,1)} copy(bf16[4,128]{1,0:T(4,128)(2,1)} %shard_map.172) | data formatting | bytes 2048

commit v3 on v2

v3 whole, which is shorter than its diff:
```python
import functools

import jax
import jax.numpy as jnp
import numpy as np
from jax import lax
from jax.experimental import pallas as pl
from jax.experimental.pallas import tpu as pltpu
from jax.sharding import PartitionSpec as P

D = 4096
EPS = 1e-06
KV = 16
ZS = 16
DK = 256
DV = 512
FU = 704
FP = 768
MSG = 1664
UPTO = 99
LIMIT = 56500000
F32 = jnp.float32
BF16 = jnp.bfloat16
MESH = pl.DeviceIdType.MESH

PLANE = sorted(
    [(dy, dx) for dy in range(4) for dx in range(4) if (dy, dx) != (0, 0)],
    key=lambda o: -(min(o[0], 4 - o[0]) + min(o[1], 4 - o[1])),
)


def dot(a, b):
    return jnp.dot(a, b, preferred_element_type=F32)


def dot_t(a, b):
    return lax.dot_general(a, b, (((1,), (1,)), ((), ())), preferred_element_type=F32)


def sin_cos(a):
    n = jnp.floor(a * np.float32(2.0 / np.pi) + 0.5)
    r = a - n * np.float32(1.5703125)
    r = r - n * np.float32(4.837512969970703125e-4)
    r = r - n * np.float32(7.549789954891882e-8)
    z = r * r
    s = r + r * z * (-1.6666654611e-1 + z * (8.3321608736e-3 - z * 1.9515295891e-4))
    c = 1.0 - 0.5 * z + z * z * (
        4.166664568298827e-2 + z * (-1.388731625493765e-3 + z * 2.443315711809948e-5)
    )
    m = n - 4.0 * jnp.floor(n * 0.25)
    odd = (m == 1.0) | (m == 3.0)
    sine = jnp.where(odd, c, s)
    cosine = jnp.where(odd, s, c)
    sine = jnp.where(m >= 2.0, -sine, sine)
    cosine = jnp.where((m == 1.0) | (m == 2.0), -cosine, cosine)
    return sine, cosine


def kernel(
    hid, mgain, wq, wk, wv, wg, decay, state, kblk, vblk, lens, ggain, wo, cgain, hg, hu, hd, freq,
    out,
    hid_v, mg_v, w1, state_v, kb_v, vb_v, gg_v, wo_v, cg_v, w2g, w2u, wd_v, fr_v, len_s, dec_s,
    sh, sl, sin_v, cos_v, wt_v, carry_v,
    xo, xg, xs, msg, rb, mx, mgat, lhs_f, psend, pr, mid3, give, mres, msg2, rb2, act, agat, lhs_d,
    hmsg, hr,
    lsem, wss, wrs, ssa, rsa, ssb, rsb, ssc, rsc, ssd, rsd, ssm, rsm, ssf, rsf, ssg, rsg, ssh, rsh,
    far,
):
    k = lax.axis_index("kv")
    t = lax.axis_index("tp")
    z, c = t // 2, t % 2
    y, x = k // 4, k % 4
    sib = 2 * z + 1 - c
    mine = pl.ds(pl.multiple_of(c * 128, 128), 128)
    pending = []

    def kv_peer(dy, dx):
        return ((y + dy) % 4) * 4 + (x + dx) % 4

    def z_peer(i):
        off = 8 - (i + 1) // 2
        sign = (i % 2) * 2 - 1
        return (z + sign * off + 16) % 16

    def drain(n=None):
        for _ in range(len(pending) if n is None else n):
            pending.pop(0)()

    def to(src, dst, ss, rs, kv, tp):
        return pltpu.make_async_remote_copy(
            src_ref=src, dst_ref=dst, send_sem=ss, recv_sem=rs,
            device_id={"kv": kv, "tp": tp}, device_id_type=MESH,
        )

    def all_done(buf, n, sem):
        part = buf.at[pl.ds(0, n)]
        pltpu.make_async_copy(part, part, sem).wait()

    def signal(sem, kv, tp):
        pl.semaphore_signal(sem, inc=1, device_id={"kv": kv, "tp": tp}, device_id_type=MESH)

    barrier = pltpu.get_barrier_semaphore()
    for dy, dx in PLANE:
        for core in range(2):
            signal(barrier, kv_peer(dy, dx), 2 * z + core)
    for dz in (4, -4, 3, -3, 2, -2, 1, -1):
        signal(barrier, k, ((z + dz + 16) % 16) * 2 + c)
    signal(barrier, k, sib)

    loads = [
        (hid, hid_v), (lens, len_s), (decay, dec_s), (freq, fr_v), (mgain, mg_v.at[c]),
        (wq, w1.at[mine, pl.ds(0, 256)]), (wk, w1.at[mine, pl.ds(256, 256)]),
        (wv, w1.at[mine, pl.ds(512, 512)]), (wg, w1.at[mine, pl.ds(1024, 512)]),
        (state, state_v), (kblk, kb_v), (vblk, vb_v), (ggain, gg_v), (wo, wo_v.at[:, mine]),
        (cgain, cg_v.at[c]), (hg, w2g.at[:, mine]), (hu, w2u.at[:, mine]), (hd, wd_v.at[:, mine]),
    ]
    copies = [pltpu.make_async_copy(a, b, lsem.at[i]) for i, (a, b) in enumerate(loads)]
    loaded = [0] * len(loads)

    def need(*ids):
        for i in ids:
            if not loaded[i]:
                copies[i].wait()
                loaded[i] = 1

    for cp in copies:
        cp.start()
    shared = [
        (mg_v.at[c], 4), (w1.at[mine, :], (5, 6, 7, 8)), (wo_v.at[:, mine], 13), (cg_v.at[c], 14),
        (w2g.at[:, mine], 15), (w2u.at[:, mine], 16), (wd_v.at[:, mine], 17),
    ]
    share = [to(r, r, wss.at[i], wrs.at[i], k, sib) for i, (r, _) in enumerate(shared)]

    need(1, 2, 3)
    row = lax.broadcasted_iota(jnp.int32, (2, 128), 0)
    slot = lax.broadcasted_iota(jnp.int32, (2, 128), 1)
    length = jnp.where(row == 0, len_s[0], len_s[1])
    sine, cosine = sin_cos(length.astype(F32) * fr_v[...])
    sin_v[...] = sine
    cos_v[...] = cosine
    filled = length & 127
    rate = dec_s[0]
    wt_v[...] = jnp.where(
        slot < filled, jnp.exp(-rate * (filled - slot).astype(F32)), jnp.zeros((2, 128), F32)
    )
    carry_v[...] = jnp.exp(-rate * (filled + 1).astype(F32))

    need(0)
    xo[0] = hid_v[0:2, :]
    xo[1] = hid_v[2:4, :]
    pl.semaphore_wait(barrier, 39)

    def stop(value):
        drain()
        need(*range(len(loads)))
        out[...] = jnp.broadcast_to(value, (4, 128)).astype(BF16)

    def both_cores(src, dst, ss, rs):
        for dy, dx in PLANE:
            p = kv_peer(dy, dx)
            for core in range(2):
                to(src(core, p), dst.at[16 * c + k], ss, rs, p, 2 * z + core).start()
        to(src(1 - c, k), dst.at[16 * c + k], ss, rs, k, sib).start()
        pending.append(lambda: all_done(dst, 2 * KV - 1, ss))

    both_cores(lambda core, p: xo.at[core], xg, ssa, rsa)
    for sg in (4, 12):
        signal(far, k, ((z + sg) % 16) * 2 + c)
    xg[16 * c + k] = xo[c]
    for (_, ids), cp in zip(shared, share):
        need(*((ids,) if isinstance(ids, int) else ids))
        cp.start()
    pending.append(lambda: [cp.wait_send() for cp in share])

    need(9)
    for s in range(2):
        whole = state_v[s, 0]
        high = whole.astype(BF16)
        sh[s] = high
        sl[s] = (whole - high.astype(F32)).astype(BF16)
    share[0].wait_recv()
    share[1].wait_recv()

    all_done(xg, 2 * KV - 1, rsa)
    if UPTO == 1:
        pl.semaphore_wait(far, 2)
        [cp.wait_recv() for cp in share[2:]]
        return stop(xs[0:1, 0:128])
    for i in range(KV):
        xs[2 * i : 2 * i + 2, 0:128] = xg[i].astype(F32)
        xs[2 * i : 2 * i + 2, 128:256] = xg[16 + i].astype(F32)

    def both_gains(ref):
        return jnp.concatenate([ref[0], ref[1]], axis=1)

    def squares(v):
        v = v * v
        return v[:, 0:128] + v[:, 128:256]

    def lay_out(rows, dst):
        for i in range(ZS):
            dst[i] = rows[2 * i : 2 * i + 2, :].astype(BF16)

    def z_scatter(msgs, rbuf, ss, rs):
        @pl.loop(0, 15)
        def _(i):
            p = z_peer(i)
            to(msgs.at[p], rbuf.at[z], ss, rs, k, 2 * p + c).start()

        rbuf[z] = msgs[z]
        pending.append(lambda: all_done(rbuf, ZS - 1, ss))
        all_done(rbuf, ZS - 1, rs)

    def z_total(rbuf):
        total = rbuf[0].astype(F32)
        for i in range(1, ZS):
            total = total + rbuf[i].astype(F32)
        scale = lax.rsqrt(
            jnp.sum(total[:, 1536:1664], axis=1, keepdims=True) * np.float32(1.0 / D) + EPS
        )
        return total, scale

    stream = xs[...]
    scaled = (stream * both_gains(mg_v)).astype(BF16)
    lay_out(jnp.concatenate([dot(scaled, w1[...]), squares(stream)], axis=1), msg)
    pl.semaphore_wait(far, 2)
    if UPTO == 2:
        [cp.wait_recv() for cp in share[2:]]
        return stop(msg[0, :, 0:128].astype(F32)[0:1, :])
    z_scatter(msg, rb, ssb, rsb)
    total, scale = z_total(rb)

    def rounded(v):
        return (scale * v).astype(BF16).astype(F32)

    queries, keys_new = rounded(total[:, 0:256]), rounded(total[:, 256:512])
    values_new, gates = rounded(total[:, 512:1024]), rounded(total[:, 1024:1536])
    sine, cosine = sin_v[...], cos_v[...]

    def rotate(v):
        a, b = v[:, 0:128], v[:, 128:256]
        return jnp.concatenate([a * cosine - b * sine, a * sine + b * cosine], axis=1)

    rot = rotate(queries).astype(BF16)
    rot_w = rot.astype(F32)
    fresh = rotate(keys_new) * np.float32(DK**-0.5)
    need(10, 11, 12)

    def pick(a, b):
        first = lax.broadcasted_iota(jnp.int32, a.shape, 0) == 0
        return jnp.where(first, a, b)

    scores = pick(*[dot_t(rot, kb_v[s, 0]) for s in range(2)])
    bw = (scores * wt_v[...]).astype(BF16)
    block_term = pick(*[dot(bw, vb_v[s, 0]) for s in range(2)])
    state_term = pick(*[dot(rot, sh[s]) + dot(rot, sl[s]) for s in range(2)])
    own_term = jnp.sum(rot_w * fresh, axis=1, keepdims=True) * values_new
    retained = own_term + block_term + carry_v[:, 0:1] * state_term
    centre = jnp.mean(retained, axis=1, keepdims=True)
    off = retained - centre
    spread = jnp.mean(off * off, axis=1, keepdims=True)
    normed = off * lax.rsqrt(spread + EPS)
    silu = gates / (1.0 + jnp.exp(-gates))
    mx[...] = (silu * normed * gg_v[...][None, :]).astype(BF16)

    def z_gather(src, buf, ss, rs):
        @pl.loop(0, 15)
        def _(i):
            to(src, buf.at[z], ss, rs, k, 2 * z_peer(i) + c).start()

        buf[z] = src[...]
        drain()
        pending.append(lambda: all_done(buf, ZS - 1, ss))

    z_gather(mx, mgat, ssc, rsc)
    [cp.wait_recv() for cp in share[2:]]
    all_done(mgat, ZS - 1, rsc)
    if UPTO == 5:
        return stop(mgat[0, :, 0:128].astype(F32)[0:1, :])
    for i in range(ZS):
        lhs_f[2 * i : 2 * i + 2, :] = mgat[i].astype(F32)

    psend[...] = dot(lhs_f[...].astype(BF16), wo_v[...]).astype(BF16)
    for dy, dx in PLANE:
        p = kv_peer(dy, dx)
        to(psend, pr.at[k], ssd, rsd, p, t).start()
    pr[k] = psend[...]
    drain()
    pending.append(lambda: all_done(pr, KV - 1, ssd))
    all_done(pr, KV - 1, rsd)
    if UPTO == 7:
        return stop(pr[0, 0:16, 0:128].astype(F32)[0:1, :])
    middle = xs[...] + jnp.sum(pr[...].astype(F32), axis=0)
    scaled = (middle * both_gains(cg_v)).astype(BF16)
    pad = jnp.zeros((32, FP - FU), F32)
    lay_out(
        jnp.concatenate(
            [dot_t(scaled, w2g[...]), pad, dot_t(scaled, w2u[...]), pad, squares(middle)], axis=1
        ),
        msg2,
    )
    if UPTO == 8:
        return stop(msg2[0, :, 0:128].astype(F32)[0:1, :])

    def residual():
        for i in range(KV):
            mid3[i] = middle[2 * i : 2 * i + 2, :]
        rows = mid3[k]
        give[0] = rows[:, 0:128]
        give[1] = rows[:, 128:256]
        mres[c] = give[c]
        to(give.at[1 - c], mres.at[c], ssm, rsm, k, sib).start()

    @pl.loop(0, 15)
    def _(i):
        p = z_peer(i)
        to(msg2.at[p], rb2.at[z], ssf, rsf, k, 2 * p + c).start()

    rb2[z] = msg2[z]
    residual()
    drain()
    all_done(rb2, ZS - 1, rsf)
    pending.append(lambda: all_done(rb2, ZS - 1, ssf))
    other = to(give.at[1 - c], mres.at[1 - c], ssm, rsm, k, sib)
    pending.append(other.wait)
    total, scale = z_total(rb2)
    gate_part, up_part = scale * total[:, 0:FU], scale * total[:, FP : FP + FU]
    act[...] = (gate_part / (1.0 + jnp.exp(-gate_part)) * up_part).astype(BF16)
    if UPTO == 9:
        return stop(act[:, 0:128].astype(F32)[0:1, :])
    z_gather(act, agat, ssg, rsg)
    all_done(agat, ZS - 1, rsg)
    if UPTO == 10:
        return stop(agat[0, :, 0:128].astype(F32)[0:1, :])
    for i in range(ZS):
        lhs_d[2 * i : 2 * i + 2, :] = agat[i].astype(F32)

    part = dot(lhs_d[...].astype(BF16), wd_v[...])
    for i in range(KV):
        hmsg[i] = part[2 * i : 2 * i + 2, 0:128].astype(BF16)
        hmsg[16 + i] = part[2 * i : 2 * i + 2, 128:256].astype(BF16)
    both_cores(lambda core, p: hmsg.at[16 * core + p], hr, ssh, rsh)
    hr[16 * c + k] = hmsg[16 * c + k]
    drain(1)
    all_done(hr, 2 * KV - 1, rsh)
    for half in range(2):
        total = mres[half]
        for i in range(KV):
            total = total + hr[16 * half + i].astype(F32)
        out[2 * half : 2 * half + 2, :] = total.astype(BF16)
    drain()


def scratch():
    v = pltpu.VMEM
    dma = pltpu.SemaphoreType.DMA
    return [
        v((4, 128), BF16), v((2, 1, 128), F32), v((256, 1536), BF16), v((2, 1, 256, 512), F32),
        v((2, 1, 128, 256), BF16), v((2, 1, 128, 512), BF16), v((512,), F32), v((512, 256), BF16),
        v((2, 1, 128), F32), v((FU, 256), BF16), v((FU, 256), BF16), v((FU, 256), BF16),
        v((1, 128), F32), pltpu.SMEM((2,), jnp.int32), pltpu.SMEM((1,), F32),
        v((2, 256, 512), BF16), v((2, 256, 512), BF16),
        v((2, 128), F32), v((2, 128), F32), v((2, 128), F32), v((2, 128), F32),
        v((2, 2, 128), BF16), v((2 * KV, 2, 128), BF16), v((32, 256), F32),
        v((ZS, 2, MSG), BF16), v((ZS, 2, MSG), BF16), v((2, DV), BF16), v((ZS, 2, DV), BF16),
        v((32, DV), F32), v((32, 256), BF16), v((KV, 32, 256), BF16), v((KV, 2, 256), F32),
        v((2, 2, 128), F32), v((2, 2, 128), F32), v((ZS, 2, MSG), BF16), v((ZS, 2, MSG), BF16),
        v((2, FU), BF16), v((ZS, 2, FU), BF16), v((32, FU), F32),
        v((2 * KV, 2, 128), BF16), v((2 * KV, 2, 128), BF16),
        dma((18,)), dma((7,)), dma((7,)), *[dma] * 16, pltpu.SemaphoreType.REGULAR,
    ]


def local(*args):
    freq = jnp.asarray(
        (10000.0 ** (-np.arange(128, dtype=np.float64) / 128)).astype(np.float32)[None, :]
    )
    args = list(args)
    for i in (1, 13):
        args[i] = args[i].reshape(1, 128)
    for i in (14, 15):
        args[i] = args[i].T
    return pl.pallas_call(
        kernel,
        out_shape=jax.ShapeDtypeStruct((4, 128), BF16),
        in_specs=[pl.BlockSpec(memory_space=pltpu.HBM)] * 18,
        out_specs=pl.BlockSpec(memory_space=pltpu.VMEM),
        scratch_shapes=scratch(),
        compiler_params=pltpu.CompilerParams(
            collective_id=0, has_side_effects=True, vmem_limit_bytes=LIMIT
        ),
    )(*args, freq)


def solution(mesh):
    in_specs = (
        P("kv", "tp"), P("tp"), P("tp", "kv"), P("tp", "kv"), P("tp", "kv"), P("tp", "kv"),
        P("kv"), P("tp", "kv", None, None), P("tp", "kv", None, None), P("tp", "kv", None, None),
        P("tp"), P("kv"), P("kv", "tp"), P("tp"), P("tp", "kv"), P("tp", "kv"), P("kv", "tp"),
    )
    return jax.shard_map(
        local, mesh=mesh, in_specs=in_specs, out_specs=P("kv", "tp"), check_vma=False
    )
```

time: 68.1 us -> 62.8 us (0.922)
  Pallas kernels: 66 us -> 60.7 us
    pallas_call x1, Pallas kernels: 66 us -> 60.7 us  [local(): pl.pallas_call(kernel, out_shape=jax.ShapeDtypeStruct((4, 128), BF16), in...]
where the time goes in v3:
time: 62.8 us; the launch traced here: 62.7 us
  Pallas kernels  60.7 us (97%)
  local copies, waits for them, and re-layouts  1.26 us (2%)
  between operations  0.71 us (1%)
    pallas_call x1, Pallas kernels, local(): pl.pallas_call(kernel, out_shape=jax.ShapeDtypeStruct((4, 128), BF16), in...  60.7 us
    unnamed x13, local copies, waits for them, and re-layouts  1.26 us

profile of v3, /device:TPU:1, one launch (start us, length us, event | category | flops | bytes accessed | tf_op | source)
XLA Modules:
  0.0 62.7 jit_solution(7484150394461076430)
XLA Ops:
  0.7 0.0 copy-start.3
  0.7 0.0 copy-start.4
  0.7 0.0 copy-start.5
  0.7 0.0 copy-start
  0.7 0.0 copy-start.1
  0.7 0.0 copy-start.2
  0.7 0.6 copy-done.3
  1.3 0.0 copy-done.4
  1.3 0.0 copy-done.5
  1.3 0.0 copy-done
  1.4 0.0 copy-done.1
  1.4 0.0 copy-done.2
  1.4 60.7 %shard_map.172 = bf16[4,128]{1,0:T(4,128)(2,1)S(1)} custom-call(bf16[4,128]{1,0:T(4,128)(2,1)S(1)} %copy-done.1, f32[1,128]{1,0:T(1,128)S(1)} %bitcast.4, bf16[128,256]{1,0:T(8,128)(2,1)} %wq.1, bf16[128,256]{1,0:T(8,128)(2,1)} %wk.1, bf16[128,512]{1,0:T(8,128)(2,1)} %wv.1, bf16[128,512]{1,0:T(8,128)(2,1)} %wg.1, f32[1]{0:T(128)S(6)} %copy.20.decay, ...), custom_call_target="tpu_custom_call" | custom-call | tf_op jit(solution)/shard_map/pallas_call | solution.py:383
  62.1 0.6 copy.21
Async XLA Ops:
  0.7 0.7 %copy-start.3 = (s32[2]{0:T(128)S(1)}, s32[2]{0:T(128)}, u32[]{:S(2)}) copy-start(s32[2]{0:T(128)} %lens.1) | copy-start | bytes 28
  0.7 0.7 %copy-start.4 = (f32[128]{0:T(128)S(1)}, f32[128]{0:T(128)}, u32[]{:S(2)}) copy-start(f32[128]{0:T(128)} %param.31) | copy-start | bytes 1540
  0.7 0.7 %copy-start.5 = (f32[1,128]{1,0:T(1,128)S(1)}, f32[1,128]{1,0:T(1,128)}, u32[]{:S(2)}) copy-start(f32[1,128]{1,0:T(1,128)} %constant.2.clone.freq) | copy-start | bytes 1540
  0.7 0.7 %copy-start = (f32[512]{0:T(512)S(1)}, f32[512]{0:T(512)}, u32[]{:S(2)}) copy-start(f32[512]{0:T(512)} %ggain.1) | copy-start | bytes 6148
  0.7 0.7 %copy-start.1 = (bf16[4,128]{1,0:T(4,128)(2,1)S(1)}, bf16[4,128]{1,0:T(4,128)(2,1)}, u32[]{:S(2)}) copy-start(bf16[4,128]{1,0:T(4,128)(2,1)} %hid.1) | copy-start | bytes 3076
  0.7 0.7 %copy-start.2 = (f32[128]{0:T(128)S(1)}, f32[128]{0:T(128)}, u32[]{:S(2)}) copy-start(f32[128]{0:T(128)} %param.19) | copy-start | bytes 1540

commit v4 on v3

--- a/solution.py
+++ b/solution.py
@@ -17,8 +17,9 @@
 FU = 704
 FP = 768
 MSG = 1664
+MSG2 = 1536
 UPTO = 99
-LIMIT = 56500000
+LIMIT = 58000000
 F32 = jnp.float32
 BF16 = jnp.bfloat16
 MESH = pl.DeviceIdType.MESH
@@ -211,12 +212,12 @@
         pending.append(lambda: all_done(rbuf, ZS - 1, ss))
         all_done(rbuf, ZS - 1, rs)
 
-    def z_total(rbuf):
+    def z_total(rbuf, first, last):
         total = rbuf[0].astype(F32)
         for i in range(1, ZS):
             total = total + rbuf[i].astype(F32)
         scale = lax.rsqrt(
-            jnp.sum(total[:, 1536:1664], axis=1, keepdims=True) * np.float32(1.0 / D) + EPS
+            jnp.sum(total[:, first:last], axis=1, keepdims=True) * np.float32(1.0 / D) + EPS
         )
         return total, scale
 
@@ -228,7 +229,7 @@
         [cp.wait_recv() for cp in share[2:]]
         return stop(msg[0, :, 0:128].astype(F32)[0:1, :])
     z_scatter(msg, rb, ssb, rsb)
-    total, scale = z_total(rb)
+    total, scale = z_total(rb, 1536, 1664)
 
     def rounded(v):
         return (scale * v).astype(BF16).astype(F32)
@@ -293,9 +294,11 @@
     middle = xs[...] + jnp.sum(pr[...].astype(F32), axis=0)
     scaled = (middle * both_gains(cg_v)).astype(BF16)
     pad = jnp.zeros((32, FP - FU), F32)
+    folded = squares(middle)
+    folded = folded[:, 0:64] + folded[:, 64:128]
     lay_out(
         jnp.concatenate(
-            [dot_t(scaled, w2g[...]), pad, dot_t(scaled, w2u[...]), pad, squares(middle)], axis=1
+            [dot_t(scaled, w2g[...]), folded, dot_t(scaled, w2u[...]), pad], axis=1
         ),
         msg2,
     )
@@ -323,7 +326,7 @@
     pending.append(lambda: all_done(rb2, ZS - 1, ssf))
     other = to(give.at[1 - c], mres.at[1 - c], ssm, rsm, k, sib)
     pending.append(other.wait)
-    total, scale = z_total(rb2)
+    total, scale = z_total(rb2, FU, FP)
     gate_part, up_part = scale * total[:, 0:FU], scale * total[:, FP : FP + FU]
     act[...] = (gate_part / (1.0 + jnp.exp(-gate_part)) * up_part).astype(BF16)
     if UPTO == 9:
@@ -364,7 +367,7 @@
         v((2, 2, 128), BF16), v((2 * KV, 2, 128), BF16), v((32, 256), F32),
         v((ZS, 2, MSG), BF16), v((ZS, 2, MSG), BF16), v((2, DV), BF16), v((ZS, 2, DV), BF16),
         v((32, DV), F32), v((32, 256), BF16), v((KV, 32, 256), BF16), v((KV, 2, 256), F32),
-        v((2, 2, 128), F32), v((2, 2, 128), F32), v((ZS, 2, MSG), BF16), v((ZS, 2, MSG), BF16),
+        v((2, 2, 128), F32), v((2, 2, 128), F32), v((ZS, 2, MSG2), BF16), v((ZS, 2, MSG2), BF16),
         v((2, FU), BF16), v((ZS, 2, FU), BF16), v((32, FU), F32),
         v((2 * KV, 2, 128), BF16), v((2 * KV, 2, 128), BF16),
         dma((18,)), dma((7,)), dma((7,)), *[dma] * 16, pltpu.SemaphoreType.REGULAR,
@@ -382,7 +385,7 @@
         args[i] = args[i].T
     return pl.pallas_call(
         kernel,
-        out_shape=jax.ShapeDtypeStruct((4, 128), BF16),
+        out_shape=pltpu.VMEM((4, 128), BF16),
         in_specs=[pl.BlockSpec(memory_space=pltpu.HBM)] * 18,
         out_specs=pl.BlockSpec(memory_space=pltpu.VMEM),
         scratch_shapes=scratch(),

time: 62.8 us -> 62.2 us (level)
  local copies, waits for them, and re-layouts: 1.26 us -> 0.56 us
    unnamed x13 -> x1, local copies, waits for them, and re-layouts: 1.26 us -> 0.56 us
where the time goes in v4:
time: 62.2 us; the launch traced here: 62.1 us
  Pallas kernels  60.8 us (98%)
  between operations  0.66 us (1%)
    pallas_call x1, Pallas kernels, local(): pl.pallas_call(kernel, out_shape=pltpu.VMEM((4, 128), BF16), in_specs=[pl...  60.8 us

profile of v4, /device:TPU:1, one launch (start us, length us, event | category | flops | bytes accessed | tf_op | source)
XLA Modules:
  0.0 62.1 jit_solution(9367168382760692207)
XLA Ops:
  0.7 60.8 %shard_map.172 = bf16[4,128]{1,0:T(4,128)(2,1)S(1)} custom-call(bf16[4,128]{1,0:T(4,128)(2,1)} %hid.1, f32[1,128]{1,0:T(1,128)} %bitcast.6, bf16[128,256]{1,0:T(8,128)(2,1)} %wq.1, bf16[128,256]{1,0:T(8,128)(2,1)} %wk.1, bf16[128,512]{1,0:T(8,128)(2,1)} %wv.1, bf16[128,512]{1,0:T(8,128)(2,1)} %wg.1, f32[1]{0:T(128)S(6)} %copy.21.decay, ...), custom_call_target="tpu_custom_call" | custom-call | tf_op jit(solution)/shard_map/pallas_call | solution.py:386
  61.5 0.6 copy.20
